TPU v7x, 32 devices: a whole 2x2x4 slice. The times are simulated.
32 devices in a mesh: tp: 8 (over z, x), dp: 4 (over y, core).
Axes of the slice: x: 2, y: 2, z: 4, core: 2. Of those that a mesh axis runs over, the one named last changes fastest.
Arguments:
- tokens: bfloat16 [112, 4096], P('tp', 'dp'), may hold values from -6 to 6
- w_query: bfloat16 [2, 4096, 4096], P(None, 'dp', 'tp'), may hold values from -0.09375 to 0.09375
- w_key: bfloat16 [2, 4096, 4096], P(None, 'dp', 'tp'), may hold values from -0.09375 to 0.09375
- w_value: bfloat16 [2, 4096, 4096], P(None, 'dp', 'tp'), may hold values from -0.09375 to 0.09375
- w_outgate: bfloat16 [2, 4096, 4096], P(None, 'dp', 'tp'), may hold values from -0.09375 to 0.09375
- w_ingate: bfloat16 [2, 4096, 32], P(None, 'dp'), may hold values from -0.09375 to 0.09375
- w_forget: bfloat16 [2, 4096, 32], P(None, 'dp'), may hold values from -0.09375 to 0.09375
- forget_bias: float32 [2, 32], P(None, 'tp'), may hold values from -2 to 3
- head_gain: float32 [2, 32, 128], P(None, 'tp'), may hold values from 0.1 to 1.9
- w_proj: bfloat16 [2, 4096, 4096], P(None, 'tp', 'dp'), may hold values from -0.09375 to 0.09375
- mem_matrix: float32 [2, 112, 32, 128, 128], P(None, 'dp', 'tp'), may hold values from -0.8 to 0.8
- mem_norm: float32 [2, 112, 32, 128], P(None, 'dp', 'tp'), may hold values from -1.2 to 1.2
- mem_max: float32 [2, 112, 32], P(None, 'dp', 'tp'), may hold values from -4 to 4
Outputs:
- result: bfloat16 [112, 4096], P('tp', 'dp')
- new_matrix: float32 [2, 112, 32, 128, 128], P(None, 'dp', 'tp')
- new_norm: float32 [2, 112, 32, 128], P(None, 'dp', 'tp')
- new_max: float32 [2, 112, 32], P(None, 'dp', 'tp')
All inputs are finite; a program needn't handle non-finite values.
Results may differ from a plain program's by a relative error of at most 0.017.
Values may be sent and summed in bfloat16 or wider, within the bound.
No kernel may reach another device: no remote copies, remote signals or barrier semaphores. Data moves between devices by JAX's collectives and lax.ppermute only.
A program may use at most 128 MiB of HBM per device.

v0:
```python
import jax
import jax.numpy as jnp
from jax import lax
from jax.sharding import PartitionSpec as P

HEAD = 128


norm_eps = 1e-06
head_eps = 1e-05


def cell_update(queries, key_vecs, values, log_in, log_forget, matrix, normvec, maxval):
    max_next = jnp.maximum(log_forget + maxval, log_in)
    decays = jnp.exp(log_forget + maxval - max_next)
    weight_in = jnp.exp(log_in - max_next)
    matrix_new = (
        decays[..., None, None] * matrix
        + weight_in[..., None, None] * key_vecs[..., :, None] * values[..., None, :]
    )
    norm_new = decays[..., None] * normvec + weight_in[..., None] * key_vecs
    numerator = jnp.einsum("bhd,bhde->bhe", queries, matrix_new, precision=lax.Precision.HIGHEST)
    denominator = jnp.maximum(jnp.abs(jnp.sum(queries * norm_new, axis=-1)), 1.0)
    return (numerator / denominator[..., None], matrix_new, norm_new, max_next)


def head_norm(readout, gain, outgate):
    average = jnp.mean(readout, axis=-1, keepdims=True)
    variance = jnp.mean(jnp.square(readout - average), axis=-1, keepdims=True)
    normed = (readout - average) * lax.rsqrt(variance + head_eps) * gain
    return normed * jax.nn.sigmoid(outgate)


def mix_block(gathered, weights, states):
    w_query, w_key, w_value, w_outgate, w_ingate, w_forget, bias, gain, w_proj = weights
    matrix, normvec, maxval = states
    features = gathered.shape[1] * lax.axis_size("dp")
    squares = jnp.sum(jnp.square(gathered.astype(jnp.float32)), axis=1)
    heads_dev = bias.shape[0]
    head_start = lax.axis_index("tp") * heads_dev
    gate_in = lax.dynamic_slice_in_dim(w_ingate, head_start, heads_dev, 1)
    gate_forget = lax.dynamic_slice_in_dim(w_forget, head_start, heads_dev, 1)
    part_query = jnp.dot(gathered, w_query, preferred_element_type=jnp.float32)
    part_key = jnp.dot(gathered, w_key, preferred_element_type=jnp.float32)
    part_value = jnp.dot(gathered, w_value, preferred_element_type=jnp.float32)
    part_outgate = jnp.dot(gathered, w_outgate, preferred_element_type=jnp.float32)
    part_ingate = jnp.dot(gathered, gate_in, preferred_element_type=jnp.float32)
    part_forget = jnp.dot(gathered, gate_forget, preferred_element_type=jnp.float32)
    rows_dev = gathered.shape[0] // lax.axis_size("dp")
    totals = lax.psum(squares, "dp")
    own_sum = lax.dynamic_slice_in_dim(totals, lax.axis_index("dp") * rows_dev, rows_dev, 0)
    sum_query, sum_key, sum_value, sum_outgate, sum_ingate, sum_forget = (
        lax.psum_scatter(part_query, "dp", scatter_dimension=0, tiled=True),
        lax.psum_scatter(part_key, "dp", scatter_dimension=0, tiled=True),
        lax.psum_scatter(part_value, "dp", scatter_dimension=0, tiled=True),
        lax.psum_scatter(part_outgate, "dp", scatter_dimension=0, tiled=True),
        lax.psum_scatter(part_ingate, "dp", scatter_dimension=0, tiled=True),
        lax.psum_scatter(part_forget, "dp", scatter_dimension=0, tiled=True),
    )
    inv_scale = lax.rsqrt(own_sum / features + norm_eps)[:, None]
    head_shape = (rows_dev, heads_dev, HEAD)
    queries = (sum_query * inv_scale).reshape(head_shape)
    key_vecs = (sum_key * inv_scale * HEAD ** (-0.5)).reshape(head_shape)
    values = (sum_value * inv_scale).reshape(head_shape)
    outgate = (sum_outgate * inv_scale).reshape(head_shape)
    log_in = sum_ingate * inv_scale
    log_forget = jax.nn.log_sigmoid(sum_forget * inv_scale + bias[None, :])
    readout, matrix_new, norm_new, max_next = cell_update(
        queries, key_vecs, values, log_in, log_forget, matrix, normvec, maxval
    )
    hidden = head_norm(readout, gain[None], outgate).reshape(rows_dev, -1).astype(jnp.bfloat16)
    out_partial = jnp.dot(
        lax.all_gather(hidden, "dp", axis=0, tiled=True), w_proj, preferred_element_type=jnp.float32
    )
    return (out_partial, matrix_new, norm_new, max_next)


def on_device(
    tokens,
    w_query,
    w_key,
    w_value,
    w_outgate,
    w_ingate,
    w_forget,
    forget_bias,
    head_gain,
    w_proj,
    mem_matrix,
    mem_norm,
    mem_max,
):
    current = lax.all_gather(tokens, "tp", axis=0, tiled=True)
    matrix_list, norm_list, max_list = ([], [], [])
    block_total = w_query.shape[0]
    result = current
    for block_id in range(block_total):
        weights = (
            w_query[block_id],
            w_key[block_id],
            w_value[block_id],
            w_outgate[block_id],
            w_ingate[block_id],
            w_forget[block_id],
            forget_bias[block_id],
            head_gain[block_id],
            w_proj[block_id],
        )
        out_partial, matrix_out, norm_out, max_out = mix_block(
            current, weights, (mem_matrix[block_id], mem_norm[block_id], mem_max[block_id])
        )
        matrix_list.append(matrix_out)
        norm_list.append(norm_out)
        max_list.append(max_out)
        if block_id + 1 < block_total:
            current = lax.psum(out_partial, "tp").astype(jnp.bfloat16)
        else:
            result = lax.psum_scatter(
                out_partial.astype(jnp.bfloat16), "tp", scatter_dimension=0, tiled=True
            )
    return (result, jnp.stack(matrix_list), jnp.stack(norm_list), jnp.stack(max_list))


def solution(mesh):
    in_specs = (
        P("tp", "dp"),
        P(None, "dp", "tp"),
        P(None, "dp", "tp"),
        P(None, "dp", "tp"),
        P(None, "dp", "tp"),
        P(None, "dp", None),
        P(None, "dp", None),
        P(None, "tp"),
        P(None, "tp", None),
        P(None, "tp", "dp"),
        P(None, "dp", "tp", None, None),
        P(None, "dp", "tp", None),
        P(None, "dp", "tp"),
    )
    out_specs = (
        P("tp", "dp"),
        P(None, "dp", "tp", None, None),
        P(None, "dp", "tp", None),
        P(None, "dp", "tp"),
    )
    return jax.shard_map(
        on_device, mesh=mesh, in_specs=in_specs, out_specs=out_specs, check_vma=False
    )
```

profile of v0, /device:TPU:0, one launch (start us, length us, event | category | flops | bytes accessed | tf_op | source)
XLA Modules:
  0.0 243.8 jit_solution(15858441146114237513)
XLA Ops:
  0.7 32.9 %all-gather = bf16[8,14,1024]{2,1,0:T(8,128)(2,1)S(1)} all-gather(bf16[1,14,1024]{2,1,0:T(8,128)(2,1)} %bitcast.149), channel_id=1, replica_groups=mesh['tp'=8,'dp'=4] {'tp'}, dimensions={0}, use_global_device_ids=true | all-gather | bytes 258048 | tf_op jit(solution)/shard_map/all_gather | solution.py:93
  35.2 1.5 fusion.38
  38.2 2.4 fusion.42
  40.6 14.0 %fusion.93 = (f32[32,512]{1,0:T(8,128)S(1)}, f32[32,512]{1,0:T(8,128)S(1)}, f32[32,512]{1,0:T(8,128)S(1)}, f32[32,512]{1,0:T(8,128)S(1)}) fusion(f32[112,512]{1,0:T(8,128)S(1)} %fusion.36, f32[112,512]{1,0:T(8,128)} %fusion.42, f32[112,512]{1,0:T(8,128)S(1)} %fusion.38, f32[112,512]{1,0:T(8,128)S(1)} %fusion.40), kind=kCustom, calls=%all-reduce-scatter.10 | all-reduce-scatter fusion | flops 262145 | bytes 1180160
  55.9 3.7 %collective-permute-start.2 = (f32[12,512]{1,0:T(8,128)S(1)}, f32[12,512]{1,0:T(8,128)S(1)}, u32[]{:S(2)}, u32[]{:S(2)}) collective-permute-start(f32[12,512]{1,0:T(8,128)S(1)} %slice.98), channel_id=1, source_target_pairs={{0,1},{1,2},{2,3},{4,5},{5,6},{6,7},{8,9},{9,10},{10,11},{12,13},{... | collective-permute-start | bytes 73736
  59.6 1.9 collective-permute-start
  61.6 1.9 collective-permute-start.3
  68.1 5.8 %all-reduce.23 = (f32[112]{0:T(128)S(1)}, f32[112,4]{0,1:T(4,128)S(1)}, f32[112,4]{0,1:T(4,128)S(1)}) all-reduce(f32[112]{0:T(128)S(1)} %multiply_reduce_fusion.1, f32[112,4]{0,1:T(4,128)S(1)} %convolution_bitcast_fusion.1, f32[112,4]{0,1:T(4,128)S(1)} %convolution_bitcast_fusion), channel_id=1, replica_groups=mesh['tp'=8,'dp'=4] {'dp'}, use_global_device_ids=true, to_apply=%region_2.0 | all-reduce | flops 1008 | bytes 8064 | tf_op jit(solution)/shard_map/psum | solution.py:50
  79.7 9.2 %fusion.13 = f32[28,4,1,128]{3,2,1,0:T(1,128)S(1)} fusion(f32[28,4,128,1]{2,3,1,0:T(1,128)S(1)} %bitcast.148, f32[2,28,4,128,128]{4,3,2,1,0:T(8,128)} %param.23, f32[28,4,128]{2,1,0:T(4,128)S(1)} %mul.321, f32[28,4,128]{2,1,0:T(4,128)S(1)} %get-tuple-element.37, f32[28,4]{1,0:T(8,128)S(1)} %copy.41), kind=kOutput, calls=%fused_computation.6 | convolution fusion | flops 27525120 | bytes 7569856 | tf_op jit(solution)/shard_map/bhd,bhde->bhe/dot_general | solution.py:22
  89.4 5.4 %all-gather.1 = bf16[4,28,512]{2,1,0:T(8,128)(2,1)S(1)} all-gather(bf16[1,28,512]{2,1,0:T(8,128)(2,1)S(1)} %reshape.136), channel_id=1, replica_groups=mesh['tp'=8,'dp'=4] {'dp'}, dimensions={0}, use_global_device_ids=true | all-gather | bytes 143360 | tf_op jit(solution)/shard_map/all_gather | solution.py:73
  95.2 43.0 %all-reduce.27 = bf16[112,1024]{1,0:T(8,128)(2,1)S(1)} all-reduce(f32[112,1024]{1,0:T(8,128)S(1)} %fusion.34), channel_id=1, replica_groups=mesh['tp'=8,'dp'=4] {'tp'}, use_global_device_ids=true, to_apply=%region_11.12 | all-reduce | flops 114688 | bytes 688128 | tf_op jit(solution)/shard_map/psum | solution.py:116
  139.9 1.5 fusion.30
  144.8 5.7 %all-reduce.22 = (f32[112]{0:T(128)S(1)}, f32[112,4]{0,1:T(4,128)S(1)}, f32[112,4]{0,1:T(4,128)S(1)}) all-reduce(f32[112]{0:T(128)S(1)} %multiply_reduce_fusion, f32[112,4]{0,1:T(4,128)S(1)} %fusion.72, f32[112,4]{0,1:T(4,128)S(1)} %fusion.70), channel_id=1, replica_groups=mesh['tp'=8,'dp'=4] {'dp'}, use_global_device_ids=true, to_apply=%region_14.15 | all-reduce | flops 1008 | bytes 8064 | tf_op jit(solution)/shard_map/psum | solution.py:50
  150.9 14.6 %fusion.92 = (f32[32,512]{1,0:T(8,128)S(1)}, f32[32,512]{1,0:T(8,128)S(1)}, f32[32,512]{1,0:T(8,128)S(1)}, f32[32,512]{1,0:T(8,128)S(1)}) fusion(f32[112,512]{1,0:T(8,128)S(1)} %fusion.26, f32[112,512]{1,0:T(8,128)S(1)} %fusion.32, f32[112,512]{1,0:T(8,128)S(1)} %fusion.28, f32[112,512]{1,0:T(8,128)S(1)} %fusion.30), kind=kCustom, calls=%all-reduce-scatter.9 | all-reduce-scatter fusion | flops 262145 | bytes 1180160
  166.8 3.8 %collective-permute-start.6 = (f32[12,512]{1,0:T(8,128)S(1)}, f32[12,512]{1,0:T(8,128)S(1)}, u32[]{:S(2)}, u32[]{:S(2)}) collective-permute-start(f32[12,512]{1,0:T(8,128)S(1)} %slice.102), channel_id=1, source_target_pairs={{0,1},{1,2},{2,3},{4,5},{5,6},{6,7},{8,9},{9,10},{10,11},{12,13},{... | collective-permute-start | bytes 73736
  170.6 1.9 collective-permute-start.4
  172.6 2.1 collective-permute-start.7
  176.8 14.1 %multiply_add_fusion.1 = (f32[1,28,4,128,128]{4,3,2,1,0:T(8,128)}, f32[1,28,4,128,128]{4,3,2,1,0:T(8,128)}) fusion(f32[2,28,4,128,128]{4,3,2,1,0:T(8,128)} %param.23, f32[28,4,128]{2,1,0:T(4,128)S(1)} %mul.321, f32[28,4,128]{2,1,0:T(4,128)S(1)} %get-tuple-element.37, f32[28,4]{1,0:T(8,128)S(1)} %copy.41, f32[28,4,128]{2,1,0:T(4,128)S(1)} %mul.347, ...), kind=kLoop, calls=%fused_computation.8 | loop fusion | flops 11010048 | bytes 29590400 | tf_op jit(solution)/shard_map/add | solution.py:18
  190.9 6.9 %fusion.10 = f32[28,4,1,128]{3,2,1,0:T(1,128)S(1)} fusion(f32[28,4,128,1]{2,3,1,0:T(1,128)S(1)} %bitcast.147, f32[2,28,4,128,128]{4,3,2,1,0:T(8,128)S(1)} %bitcast.144, f32[28,4,128]{2,1,0:T(4,128)S(1)} %mul.347, f32[28,4,128]{2,1,0:T(4,128)S(1)} %get-tuple-element.33, f32[28,4]{1,0:T(8,128)S(1)} %copy.44), kind=kOutput, calls=%fused_computation.3 | convolution fusion | flops 27525120 | bytes 7585792 | tf_op jit(solution)/shard_map/bhd,bhde->bhe/dot_general | solution.py:22
  198.4 5.4 %all-gather.2 = bf16[4,28,512]{2,1,0:T(8,128)(2,1)S(1)} all-gather(bf16[1,28,512]{2,1,0:T(8,128)(2,1)S(1)} %reshape.138), channel_id=1, replica_groups=mesh['tp'=8,'dp'=4] {'dp'}, dimensions={0}, use_global_device_ids=true | all-gather | bytes 143360 | tf_op jit(solution)/shard_map/all_gather | solution.py:73
  203.9 1.5 convolution_convert_fusion
  205.4 21.2 %fusion.8 = bf16[16,1024]{1,0:T(8,128)(2,1)S(1)} fusion(bf16[112,1024]{1,0:T(8,128)(2,1)S(1)} %convolution_convert_fusion), kind=kCustom, calls=%all-reduce-scatter.8 | all-reduce-scatter fusion | flops 131073 | bytes 262656
  226.6 2.1 collective-permute-start.8
  228.9 13.4 %pad_maximum_fusion = f32[2,28,4,128,128]{4,3,2,1,0:T(8,128)} fusion(f32[1,28,4,128,128]{4,3,2,1,0:T(8,128)} %get-tuple-element.39, f32[1,28,4,128,128]{4,3,2,1,0:T(8,128)} %get-tuple-element.38), kind=kLoop, calls=%fused_computation | loop fusion | flops 3670016 | bytes 29360128 | tf_op jit(solution)/shard_map/stack | solution.py:121
  (113 shorter events, 24.4 us)
Async XLA Ops:
  0.6 64.3 %copy-start.2 = (bf16[2,1024,32]{1,2,0:T(8,128)(2,1)S(1)}, bf16[2,1024,32]{1,2,0:T(8,128)(2,1)}, u32[]{:S(2)}) copy-start(bf16[2,1024,32]{1,2,0:T(8,128)(2,1)} %param.18) | copy-start | bytes 393220
  0.6 78.8 %copy-start.1 = (f32[2,28,4,128]{3,2,1,0:T(4,128)S(1)}, f32[2,28,4,128]{3,2,1,0:T(4,128)}, u32[]{:S(2)}) copy-start(f32[2,28,4,128]{3,2,1,0:T(4,128)} %param.24) | copy-start | bytes 344068
  38.2 56.7 %copy-start = (bf16[2,512,1024]{2,1,0:T(8,128)(2,1)S(1)}, bf16[2,512,1024]{2,1,0:T(8,128)(2,1)}, u32[]{:S(2)}) copy-start(bf16[2,512,1024]{2,1,0:T(8,128)(2,1)} %param.22) | copy-start | bytes 6291460
  54.6 23.8 %collective-permute-start.1 = (f32[12,512]{1,0:T(8,128)S(1)}, f32[12,512]{1,0:T(8,128)S(1)}, u32[]{:S(2)}, u32[]{:S(2)}) collective-permute-start(f32[12,512]{1,0:T(8,128)S(1)} %slice.97), channel_id=1, source_target_pairs={{0,1},{1,2},{2,3},{4,5},{5,6},{6,7},{8,9},{9,10},{10,11},{12,13},{... | collective-permute-start | bytes 73736
  55.9 22.6 %collective-permute-start.2 = (f32[12,512]{1,0:T(8,128)S(1)}, f32[12,512]{1,0:T(8,128)S(1)}, u32[]{:S(2)}, u32[]{:S(2)}) collective-permute-start(f32[12,512]{1,0:T(8,128)S(1)} %slice.98), channel_id=1, source_target_pairs={{0,1},{1,2},{2,3},{4,5},{5,6},{6,7},{8,9},{9,10},{10,11},{12,13},{... | collective-permute-start | bytes 73736
  59.6 19.2 %collective-permute-start = (f32[12,512]{1,0:T(8,128)S(1)}, f32[12,512]{1,0:T(8,128)S(1)}, u32[]{:S(2)}, u32[]{:S(2)}) collective-permute-start(f32[12,512]{1,0:T(8,128)S(1)} %slice.96), channel_id=1, source_target_pairs={{0,1},{1,2},{2,3},{4,5},{5,6},{6,7},{8,9},{9,10},{10,11},{12,13},{... | collective-permute-start | bytes 73736
  61.6 17.4 %collective-permute-start.3 = (f32[12,512]{1,0:T(8,128)S(1)}, f32[12,512]{1,0:T(8,128)S(1)}, u32[]{:S(2)}, u32[]{:S(2)}) collective-permute-start(f32[12,512]{1,0:T(8,128)S(1)} %slice.99), channel_id=1, source_target_pairs={{0,1},{1,2},{2,3},{4,5},{5,6},{6,7},{8,9},{9,10},{10,11},{12,13},{... | collective-permute-start | bytes 73736
  79.7 71.0 %copy-start.3 = (f32[2,28,4]{1,2,0:T(4,128)S(1)}, f32[2,28,4]{1,2,0:T(4,128)}, u32[]{:S(2)}) copy-start(f32[2,28,4]{1,2,0:T(4,128)} %param.25) | copy-start | bytes 2692
  79.7 71.0 %copy-start.4 = (f32[4]{0:T(128)S(1)}, f32[4]{0:T(128)}, u32[]{:S(2)}) copy-start(f32[4]{0:T(128)} %get-tuple-element.52) | copy-start | bytes 52
  165.5 10.0 %collective-permute-start.5 = (f32[12,512]{1,0:T(8,128)S(1)}, f32[12,512]{1,0:T(8,128)S(1)}, u32[]{:S(2)}, u32[]{:S(2)}) collective-permute-start(f32[12,512]{1,0:T(8,128)S(1)} %slice.101), channel_id=1, source_target_pairs={{0,1},{1,2},{2,3},{4,5},{5,6},{6,7},{8,9},{9,10},{10,11},{12,13},{... | collective-permute-start | bytes 73736
  166.8 8.9 %collective-permute-start.6 = (f32[12,512]{1,0:T(8,128)S(1)}, f32[12,512]{1,0:T(8,128)S(1)}, u32[]{:S(2)}, u32[]{:S(2)}) collective-permute-start(f32[12,512]{1,0:T(8,128)S(1)} %slice.102), channel_id=1, source_target_pairs={{0,1},{1,2},{2,3},{4,5},{5,6},{6,7},{8,9},{9,10},{10,11},{12,13},{... | collective-permute-start | bytes 73736
  170.6 5.2 %collective-permute-start.4 = (f32[12,512]{1,0:T(8,128)S(1)}, f32[12,512]{1,0:T(8,128)S(1)}, u32[]{:S(2)}, u32[]{:S(2)}) collective-permute-start(f32[12,512]{1,0:T(8,128)S(1)} %slice.100), channel_id=1, source_target_pairs={{0,1},{1,2},{2,3},{4,5},{5,6},{6,7},{8,9},{9,10},{10,11},{12,13},{... | collective-permute-start | bytes 73736
  172.6 3.5 %collective-permute-start.7 = (f32[12,512]{1,0:T(8,128)S(1)}, f32[12,512]{1,0:T(8,128)S(1)}, u32[]{:S(2)}, u32[]{:S(2)}) collective-permute-start(f32[12,512]{1,0:T(8,128)S(1)} %slice.103), channel_id=1, source_target_pairs={{0,1},{1,2},{2,3},{4,5},{5,6},{6,7},{8,9},{9,10},{10,11},{12,13},{... | collective-permute-start | bytes 73736
  176.5 14.4 %slice-start = ((s8[14680064]{0:T(1024)(128)(4,1)}), s8[2097152]{0:T(1024)(128)(4,1)S(1)}, s32[]{:S(2)}) async-start(s8[14680064]{0:T(1024)(128)(4,1)} %bitcast.143), calls=%async_computation | async-start | bytes 4194304
  176.8 14.1 %slice-start.1 = ((s8[14680064]{0:T(1024)(128)(4,1)}), s8[4194304]{0:T(1024)(128)(4,1)S(1)}, s32[]{:S(2)}) async-start(s8[14680064]{0:T(1024)(128)(4,1)} %bitcast.143), calls=%async_computation.1 | async-start | bytes 8388608
  176.8 14.1 %slice-start.2 = ((s8[14680064]{0:T(1024)(128)(4,1)}), s8[4194304]{0:T(1024)(128)(4,1)S(1)}, s32[]{:S(2)}) async-start(s8[14680064]{0:T(1024)(128)(4,1)} %bitcast.143), calls=%async_computation.2 | async-start | bytes 8388608
  176.8 14.1 %slice-start.3 = ((s8[14680064]{0:T(1024)(128)(4,1)}), s8[4194304]{0:T(1024)(128)(4,1)S(1)}, s32[]{:S(2)}) async-start(s8[14680064]{0:T(1024)(128)(4,1)} %bitcast.143), calls=%async_computation.3 | async-start | bytes 8388608
  226.6 16.3 %collective-permute-start.8 = (bf16[14,1024]{1,0:T(8,128)(2,1)S(1)}, bf16[14,1024]{1,0:T(8,128)(2,1)S(1)}, u32[]{:S(2)}, u32[]{:S(2)}) collective-permute-start(bf16[14,1024]{1,0:T(8,128)(2,1)S(1)} %slice.104), channel_id=1, source_target_pairs={{0,4},{4,8},{8,12},{12,16},{16,20},{20,24},{24,28},{1,5},{5,9},{9,... | collective-permute-start | bytes 86024
where the time goes:
time: 245 us; the launch traced here: 244 us
  blocking collectives  148 us (60%)
  other arithmetic  31.9 us (13%)
  matrix products  31.7 us (13%)
  starting transfers between devices  20 us (8%)
  local copies, waits for them, and re-layouts  8.64 us (4%)
  between operations  3.34 us (1%)
    unnamed x3, blocking collectives  49.8 us
    psum x1, blocking collectives, on_device(): current = lax.psum(out_partial, 'tp').astype(jnp.bfloat16)  43 us
    all_gather x1, blocking collectives, on_device(): current = lax.all_gather(tokens, 'tp', axis=0, tiled=True)  32.9 us
    unnamed x9, starting transfers between devices  20 us
    dot_general x2, matrix products, cell_update(): jnp.einsum('bhd,bhde->bhe', queries, matrix_new, precision=lax.Precision....  16.1 us
    add x1, other arithmetic, cell_update(): decays[..., None, None] * matrix  14.1 us
    another operation x1, other arithmetic, on_device(): jnp.stack(matrix_list)  13.4 us
    psum x2, blocking collectives, mix_block(): totals = lax.psum(squares, 'dp')  11.6 us
  transfers between devices with their start and end apart: 9, of which 0 were waited for; matrix products, arithmetic and copies ran while one was open for 10% of the time, Pallas kernels for 0%

commit v1 on v0

v1 whole, which is shorter than its diff:
```python
import functools

import jax
import jax.numpy as jnp
from jax import lax
from jax.experimental import pallas as pl
from jax.experimental.pallas import tpu as pltpu
from jax.sharding import PartitionSpec as P

norm_eps = 1e-06
head_eps = 1e-05
PAD = 16
LANES = 128
UP = 12.0
TINY = 1e-30
OUT_UP = 16.0
F32 = jnp.float32
BF16 = jnp.bfloat16


def lane_roll(x, amount):
    return pltpu.roll(x, amount % x.shape[-1], 1)


def project_kernel(block, heads_all, meta, x, wq, wk, wv, wo, wi, wf, own, *rest):
    sends, (x_rel, gates, wide_w, gate_w, sems) = rest[:-5], rest[-5:]
    copies = [
        pltpu.make_async_copy(source.at[block], target.at[i], sems.at[n])
        for n, (source, target, i) in enumerate(
            [(wi, gate_w, 0), (wf, gate_w, 1), (wq, wide_w, 0), (wk, wide_w, 1), (wv, wide_w, 2), (wo, wide_w, 3)]
        )
    ]
    for copy in copies:
        copy.start()
    slots = len(sends) + 1
    rows = x.shape[0] // slots
    me = meta[0]
    first_head = meta[1]
    for slot in range(slots):
        start = pl.multiple_of((me ^ slot) * rows, rows)
        x_rel[slot * rows : (slot + 1) * rows, :] = x[pl.ds(start, rows), :]
    xs = x_rel[...]
    cols = wq.shape[2]

    wide = xs.astype(F32)
    squares = jnp.sum(wide * wide, axis=1, keepdims=True)
    power = jnp.floor(0.5 * jnp.log2(squares + TINY))
    scale = jnp.exp2(UP - power)

    def emit(value, offset):
        width = value.shape[1]
        for slot, send in enumerate((own,) + tuple(sends)):
            send[:, offset : offset + width] = value[slot * rows : (slot + 1) * rows]

    gates[...] = jnp.zeros(gates.shape, F32)
    for index in range(2):
        copies[index].wait()
        value = jnp.dot(xs, gate_w[index], preferred_element_type=F32)
        gates[:, index * heads_all : (index + 1) * heads_all] = value
    lane = lax.broadcasted_iota(jnp.int32, gates.shape, 1)
    mine = pltpu.roll(gates[...], (LANES - first_head) % LANES, 1)
    mine = mine * scale
    mine = jnp.where(lane == heads_all - 1, squares * jnp.exp2(-2.0 * power), mine)
    mine = jnp.where(lane == heads_all - 2, power, mine)
    low = mine - mine.astype(BF16).astype(F32)
    emit(jnp.where(lane < LANES // 2, mine, pltpu.roll(low, LANES // 2, 1)), 4 * cols)
    for index in range(4):
        copies[2 + index].wait()
        emit(jnp.dot(xs, wide_w[index], preferred_element_type=F32) * scale, index * cols)


def project(block, meta, x, wq, wk, wv, wo, wi, wf, slots):
    rows = x.shape[0] // slots
    heads_all = wi.shape[2]
    width = 4 * wq.shape[2] + LANES
    whole = pl.BlockSpec(memory_space=pltpu.VMEM)

    return pl.pallas_call(
        functools.partial(project_kernel, block, heads_all),
        in_specs=[pl.BlockSpec(memory_space=pltpu.SMEM), whole] + [pl.BlockSpec(memory_space=pltpu.HBM)] * 6,
        out_specs=[whole] * slots,
        out_shape=[jax.ShapeDtypeStruct((rows, width), F32)] * slots,
        scratch_shapes=[
            pltpu.VMEM(x.shape, BF16),
            pltpu.VMEM((x.shape[0], LANES), F32),
            pltpu.VMEM((4,) + wq.shape[1:], BF16),
            pltpu.VMEM((2,) + wi.shape[1:], BF16),
            pltpu.SemaphoreType.DMA((6,)),
        ],
        compiler_params=pltpu.CompilerParams(vmem_limit_bytes=32 << 20),
        cost_estimate=pl.CostEstimate(
            flops=2 * x.shape[0] * x.shape[1] * width, bytes_accessed=5 << 20, transcendentals=0
        ),
        name="project",
    )(meta, x, wq, wk, wv, wo, wi, wf)


def spread(pairs, real):
    return [(slice(i * PAD, i * PAD + real), slice(i * real, (i + 1) * real)) for i in range(pairs)]


def cell_kernel(features, heads_all, peers, *refs):
    own = refs[0]
    parts = refs[1 : 1 + peers]
    bias, gain, norm, maxval, matrix = refs[1 + peers : 6 + peers]
    rest = refs[6 + peers :]
    if len(rest) > 13:
        rest = rest[2:]
    (hidden, norm_out, max_out, kw_out, v_out, dec_out) = rest[:6]
    (q_s, o_s, qw_s, n_s, nn_s, mp_s, part_s) = rest[6:]
    head = pl.program_id(0)
    heads = norm.shape[2]
    rows, real = own.shape[0], norm.shape[1]
    pairs = rows // PAD
    moves = spread(pairs, real // pairs)
    cols = heads * LANES

    @pl.when(head == 0)
    def _():
        scales, packed, squares = [], 0.0, 0.0
        for part in (own,) + tuple(parts):
            tile = part[:, 4 * cols :]
            tile = tile + lane_roll(tile, LANES // 2)
            power = tile[:, heads_all - 2 : heads_all - 1]
            scales.append(jnp.exp2(power - UP))
            packed = packed + tile * scales[-1]
            squares = squares + tile[:, heads_all - 1 : heads_all] * jnp.exp2(2.0 * power)

        def total(start, width):
            value = 0.0
            for part, scale in zip((own,) + tuple(parts), scales):
                value = value + part[:, start : start + width] * scale
            return value

        inv = lax.rsqrt(squares / features + norm_eps)
        log_in = packed[:, :heads] * inv
        raw = packed[:, heads_all : heads_all + heads] * inv + bias[0]
        log_forget = jnp.minimum(raw, 0.0) - jnp.log1p(jnp.exp(-jnp.abs(raw)))
        mp_s[...] = jnp.zeros(mp_s.shape, F32)
        for padded, plain in moves:
            mp_s[padded, :] = maxval[0, plain, :]
        carried = log_forget + mp_s[...]
        new_max = jnp.maximum(carried, log_in)
        decays = jnp.exp(carried - new_max)
        weight_in = jnp.exp(log_in - new_max)
        for padded, plain in moves:
            max_out[0, plain, :] = new_max[padded]
        n_s[...] = jnp.zeros(n_s.shape, F32)
        for h in range(heads):
            for padded, plain in moves:
                n_s[h, padded, :] = norm[0, plain, h, :]
            at = h * LANES
            q = total(at, LANES) * inv
            k = total(cols + at, LANES) * (inv * LANES ** (-0.5))
            q_s[h] = q
            v_out[h] = total(2 * cols + at, LANES) * inv
            o_s[h] = total(3 * cols + at, LANES) * inv
            dec = jnp.broadcast_to(decays[:, h : h + 1], (rows, LANES))
            dec_out[h] = dec
            kw = k * weight_in[:, h : h + 1]
            kw_out[h] = kw
            nn = dec * n_s[h] + kw
            nn_s[h] = nn
            for padded, plain in moves:
                norm_out[0, plain, h, :] = nn[padded]
        part_s[...] = jnp.zeros(part_s.shape, F32)

    q = q_s[head]
    q_t = q.T
    for padded, plain in moves:
        for row, seq in zip(range(rows)[padded], range(real)[plain]):
            column = jnp.broadcast_to(q_t[:, row : row + 1], (LANES, LANES))
            product = matrix[0, seq, 0] * column
            part_s[row * 8 : row * 8 + 8, :] = jnp.sum(product.reshape(LANES // 8, 8, LANES), axis=0)
    carried = part_s[pl.ds(0, rows, stride=8), :]
    for j in range(1, 8):
        carried = carried + part_s[pl.ds(j, rows, stride=8), :]
    kw = kw_out[head]
    scores = jnp.sum(q * kw, axis=1, keepdims=True)
    denominator = jnp.maximum(jnp.abs(jnp.sum(q * nn_s[head], axis=1, keepdims=True)), 1.0)
    readout = (dec_out[head] * carried + scores * v_out[head]) / denominator
    average = jnp.mean(readout, axis=1, keepdims=True)
    centred = readout - average
    variance = jnp.mean(centred * centred, axis=1, keepdims=True)
    normed = centred * lax.rsqrt(variance + head_eps) * gain[0, pl.ds(head, 1), :]
    hidden[...] = (normed * jax.nn.sigmoid(o_s[head])).astype(BF16)


def cell(block, own, parts, bias, gain, norm, maxval, matrix, heads_all, features, filled):
    rows = own.shape[0]
    blocks, real, heads, _ = norm.shape
    full = lambda a: pl.BlockSpec(a.shape, lambda h: (0,) * a.ndim)
    at = lambda a: pl.BlockSpec((1,) + a.shape[1:], lambda h: (block,) + (0,) * (a.ndim - 1))
    gates = jax.ShapeDtypeStruct((heads, rows, LANES), F32)
    aliased = [] if filled is None else list(filled)
    base = 6 + len(parts)
    bias = bias[:, None]
    return pl.pallas_call(
        functools.partial(cell_kernel, features, heads_all, len(parts)),
        grid=(heads,),
        in_specs=[full(own)]
        + [full(p) for p in parts]
        + [at(bias), at(gain), at(norm), at(maxval)]
        + [pl.BlockSpec((1, real, 1, LANES, LANES), lambda h: (block, 0, h, 0, 0))]
        + [pl.BlockSpec(memory_space=pl.ANY)] * len(aliased),
        out_specs=[
            pl.BlockSpec((rows, LANES), lambda h: (0, h)),
            at(norm),
            at(maxval),
            full(gates),
            full(gates),
            full(gates),
        ],
        out_shape=[
            jax.ShapeDtypeStruct((rows, heads * LANES), BF16),
            jax.ShapeDtypeStruct(norm.shape, F32),
            jax.ShapeDtypeStruct(maxval.shape, F32),
            gates,
            gates,
            gates,
        ],
        input_output_aliases={base: 1, base + 1: 2} if aliased else {},
        scratch_shapes=[pltpu.VMEM((heads, rows, LANES), F32)] * 5
        + [pltpu.VMEM((rows, heads), F32), pltpu.VMEM((rows * 8, LANES), F32)],
        compiler_params=pltpu.CompilerParams(vmem_limit_bytes=32 << 20),
        cost_estimate=pl.CostEstimate(
            flops=4 * real * heads * LANES * LANES,
            bytes_accessed=4 * real * heads * LANES * LANES,
            transcendentals=0,
        ),
        name="cell",
    )(own, *parts, bias, gain, norm, maxval, matrix, *aliased)


def update_kernel(kw, v, dec, matrix, *rest):
    out = rest[-1]
    head = pl.program_id(0)
    rows, real = kw.shape[1], matrix.shape[1]
    pairs = rows // PAD
    kw_t = kw[head].T
    for padded, plain in spread(pairs, real // pairs):
        for row, seq in zip(range(rows)[padded], range(real)[plain]):
            column = jnp.broadcast_to(kw_t[:, row : row + 1], (LANES, LANES))
            decay = dec[head, row : row + 1, :]
            out[0, seq, 0] = decay * matrix[0, seq, 0] + column * v[head, row : row + 1, :]


def update(block, kw, v, dec, matrix, filled):
    _, real, heads = matrix.shape[:3]
    full = lambda a: pl.BlockSpec(a.shape, lambda h: (0,) * a.ndim)
    one = pl.BlockSpec((1, real, 1, LANES, LANES), lambda h: (block, 0, h, 0, 0))
    aliased = [] if filled is None else [filled]
    return pl.pallas_call(
        update_kernel,
        grid=(heads,),
        in_specs=[full(kw), full(v), full(dec), one] + [pl.BlockSpec(memory_space=pl.ANY)] * len(aliased),
        out_specs=one,
        out_shape=jax.ShapeDtypeStruct(matrix.shape, F32),
        input_output_aliases={4: 0} if aliased else {},
        compiler_params=pltpu.CompilerParams(vmem_limit_bytes=32 << 20),
        cost_estimate=pl.CostEstimate(
            flops=4 * real * heads * LANES * LANES,
            bytes_accessed=8 * real * heads * LANES * LANES,
            transcendentals=0,
        ),
        name="update",
    )(kw, v, dec, matrix, *aliased)


def output_kernel(meta, w, *refs):
    parts, out = refs[:-1], refs[-1]
    rows = parts[0].shape[0]
    me = meta[0]
    value = jnp.dot(
        jnp.concatenate([part[...] for part in parts], axis=0), w[0], preferred_element_type=F32
    )
    value = value * OUT_UP
    for slot in range(len(parts)):
        start = pl.multiple_of((me ^ slot) * rows, rows)
        out[pl.ds(start, rows), :] = value[slot * rows : (slot + 1) * rows]


def output(block, meta, w, parts):
    rows = parts[0].shape[0]
    whole = pl.BlockSpec(memory_space=pltpu.VMEM)
    return pl.pallas_call(
        output_kernel,
        in_specs=[
            pl.BlockSpec(memory_space=pltpu.SMEM),
            pl.BlockSpec((1,) + w.shape[1:], lambda i: (block, 0, 0)),
        ]
        + [whole] * len(parts),
        grid=(1,),
        out_specs=whole,
        out_shape=jax.ShapeDtypeStruct((rows * len(parts), w.shape[2]), F32),
        compiler_params=pltpu.CompilerParams(vmem_limit_bytes=16 << 20),
        cost_estimate=pl.CostEstimate(
            flops=2 * rows * len(parts) * w.shape[1] * w.shape[2], bytes_accessed=1 << 20, transcendentals=0
        ),
        name="output",
    )(meta, w, *parts)


def swap(x, axis, size, bit):
    return lax.ppermute(x, axis, [(i, i ^ bit) for i in range(size)])


def on_device(
    tokens,
    w_query,
    w_key,
    w_value,
    w_outgate,
    w_ingate,
    w_forget,
    forget_bias,
    head_gain,
    w_proj,
    mem_matrix,
    mem_norm,
    mem_max,
):
    tp, dp = lax.axis_size("tp"), lax.axis_size("dp")
    real = tokens.shape[0]
    features = tokens.shape[1]
    heads = forget_bias.shape[1]
    heads_all = w_ingate.shape[2]
    assert dp & (dp - 1) == 0 and tp % dp == 0 and real <= PAD and 2 * heads_all <= LANES // 2
    meta = jnp.stack([lax.axis_index("dp"), lax.axis_index("tp") * heads]).astype(jnp.int32)

    def gather(rows):
        spread_rows = jnp.broadcast_to(rows[None], (tp,) + rows.shape)
        return lax.all_to_all(spread_rows, "tp", 0, 0).reshape(tp * PAD, features)

    current = gather(jnp.pad(tokens, ((0, PAD - real), (0, 0))))
    blocks = w_query.shape[0]
    filled, matrix_out = None, None
    for block in range(blocks):
        own, *sends = project(
            block, meta, current, w_query, w_key, w_value, w_outgate, w_ingate, w_forget, dp
        )
        parts = [
            swap(part.astype(jnp.float16), "dp", dp, slot).astype(F32) for slot, part in enumerate(sends, 1)
        ]
        hidden, norm_out, max_out, kw, v, dec = cell(
            block, own, parts, forget_bias, head_gain, mem_norm, mem_max, mem_matrix,
            heads_all, features * dp, filled,
        )
        filled = (norm_out, max_out)
        gathered = [hidden] + [swap(hidden, "dp", dp, slot) for slot in range(1, dp)]
        matrix_out = update(block, kw, v, dec, mem_matrix, matrix_out)
        partial = output(block, meta, w_proj, gathered).reshape(tp, PAD, features)
        summed = lax.all_to_all(partial.astype(jnp.float16), "tp", 0, 0)
        summed = (jnp.sum(summed.astype(F32), axis=0) * (1.0 / OUT_UP)).astype(BF16)
        if block + 1 < blocks:
            current = gather(summed)
    return (summed[:real], matrix_out, *filled)


def solution(mesh):
    in_specs = (
        P("tp", "dp"),
        P(None, "dp", "tp"),
        P(None, "dp", "tp"),
        P(None, "dp", "tp"),
        P(None, "dp", "tp"),
        P(None, "dp", None),
        P(None, "dp", None),
        P(None, "tp"),
        P(None, "tp", None),
        P(None, "tp", "dp"),
        P(None, "dp", "tp", None, None),
        P(None, "dp", "tp", None),
        P(None, "dp", "tp"),
    )
    out_specs = (
        P("tp", "dp"),
        P(None, "dp", "tp", None, None),
        P(None, "dp", "tp", None),
        P(None, "dp", "tp"),
    )
    return jax.shard_map(
        on_device, mesh=mesh, in_specs=in_specs, out_specs=out_specs, check_vma=False
    )
```

time: 245 us -> 129 us (0.53)
  blocking collectives: 148 us -> 23.9 us
  matrix products: 31.7 us -> 0 us
  other arithmetic: 31.9 us -> 1.78 us
  Pallas kernels: 0 us -> 28.4 us
  waiting for transfers between devices: 0.02 us -> 24.1 us
  local copies, waits for them, and re-layouts: 8.64 us -> 30.8 us
    psum x3 -> x0, blocking collectives: 54.6 us -> none  [the longest x1 43 us: on_device(): current = lax.psum(out_partial, 'tp').astype(jnp.bfloat16)]
    unnamed x3 -> x0, blocking collectives: 49.8 us -> none
    all_gather x3 -> x0, blocking collectives: 43.7 us -> none  [the longest x1 32.9 us: on_device(): current = lax.all_gather(tokens, 'tp', axis=0, tiled=True)]
    dot_general x16 -> x0, matrix products: 31.7 us -> none  [the longest x2 16.1 us: cell_update(): jnp.einsum('bhd,bhde->bhe', queries, matrix_new, precision=lax.Precision....]
    pallas_call x0 -> x8, Pallas kernels: none -> 28.4 us  [the longest x2 10.9 us: cell(): pl.pallas_call(functools.partial(cell_kernel, features, heads_all, len(pa...]
    unnamed x44 -> x64, local copies, waits for them, and re-layouts: 5.11 us -> 29.1 us
    all_to_all x0 -> x2, blocking collectives: none -> 23.9 us  [the longest x1 12.1 us: on_device(): summed = lax.all_to_all(partial.astype(jnp.float16), 'tp', 0, 0)]
    unnamed x9 -> x0, starting transfers between devices: 20 us -> none
  transfers between devices with their start and end apart: 9 -> 14, of which waited for: 0 -> 9; matrix products, arithmetic and copies ran while one was open for 10% -> 3% of each run, Pallas kernels for 0% -> 8%
where the time goes in v1:
time: 129 us
  local copies, waits for them, and re-layouts  30.8 us (24%)
  Pallas kernels  28.4 us (22%)
  waiting for transfers between devices  24.1 us (19%)
  blocking collectives  23.9 us (19%)
  starting transfers between devices  18.6 us (14%)
  other arithmetic  1.78 us (1%)
    unnamed x64, local copies, waits for them, and re-layouts  29.1 us
    ppermute x12, waiting for transfers between devices, swap(): return lax.ppermute(x, axis, [(i, i ^ bit) for i in range(size)])  18.5 us
    all_to_all x1, blocking collectives, on_device(): summed = lax.all_to_all(partial.astype(jnp.float16), 'tp', 0, 0)  12.1 us
    all_to_all x1, blocking collectives, gather(): return lax.all_to_all(spread_rows, 'tp', 0, 0).reshape(tp * PAD, features)  11.8 us
    pallas_call x2, Pallas kernels, cell(): pl.pallas_call(functools.partial(cell_kernel, features, heads_all, len(pa...  10.9 us
    pallas_call x2, Pallas kernels, update(): pl.pallas_call(update_kernel, grid=(heads,), in_specs=[full(kw), full(v),...  9.85 us
    ppermute x12, starting transfers between devices, swap(): return lax.ppermute(x, axis, [(i, i ^ bit) for i in range(size)])  7.75 us
    all_to_all x1, starting transfers between devices, gather(): return lax.all_to_all(spread_rows, 'tp', 0, 0).reshape(tp * PAD, features)  7.28 us
  transfers between devices with their start and end apart: 14, of which 9 were waited for; matrix products, arithmetic and copies ran while one was open for 3% of the time, Pallas kernels for 8%

profile of v1, /device:TPU:0, one launch (start us, length us, event | category | flops | bytes accessed | tf_op | source)
XLA Modules:
  0.0 128.5 jit_solution(7875971080107974813)
XLA Ops:
  2.3 7.3 %all-to-all-start = ((bf16[8,16,1024]{2,1,0:T(8,128)(2,1)}), bf16[8,16,1024]{2,1,0:T(8,128)(2,1)S(1)}, u32[]{:S(2)}, u32[]{:S(2)}) async-start(bf16[8,16,1024]{2,1,0:T(8,128)(2,1)} %broadcast_in_dim.6), calls=%async_computation | async-start | bytes 524288 | tf_op jit(solution)/shard_map/all_to_all | solution.py:333
  10.8 2.1 %copy.21.wf = bf16[2,1024,32]{2,1,0:T(8,128)(2,1)} copy(bf16[2,1024,32]{1,2,0:T(8,128)(2,1)} %param.19) | data formatting | bytes 262144 | tf_op args[6]
  12.9 5.6 %all-to-all-done = bf16[8,16,1024]{2,1,0:T(8,128)(2,1)S(1)} async-done(((bf16[8,16,1024]{2,1,0:T(8,128)(2,1)}), bf16[8,16,1024]{2,1,0:T(8,128)(2,1)S(1)}, u32[]{:S(2)}, u32[]{:S(2)}) %all-to-all-start) | async-done | bytes 262176 | tf_op jit(solution)/shard_map/all_to_all | solution.py:333
  18.5 1.6 %copy-done.4 = bf16[2,1024,512]{2,1,0:T(8,128)(2,1)S(1)} copy-done((bf16[2,1024,512]{2,1,0:T(8,128)(2,1)S(1)}, bf16[2,1024,512]{2,1,0:T(8,128)(2,1)}, u32[]{:S(2)}) %copy-start.4) | copy-done | bytes 2097176
  24.3 3.0 %project.2 = (f32[32,2176]{1,0:T(8,128)S(1)}, f32[32,2176]{1,0:T(8,128)S(1)}, f32[32,2176]{1,0:T(8,128)S(1)}, f32[32,2176]{1,0:T(8,128)S(1)}) custom-call(s32[2]{0:T(128)S(1)} %pad_add_fusion.meta, bf16[128,1024]{1,0:T(8,128)(2,1)S(1)} %bitcast.11, bf16[2,1024,512]{2,1,0:T(8,128)(2,1)S(1)} %copy-done.3, bf16[2,1024,512]{2,1,0:T(8,128)(2,1)S(1)} %copy-done.4, ...), custom_call_target="tpu_custom_call" | custom-call | flops 570425344 | bytes 5242880 | tf_op jit(solution)/shard_map/project/pallas_call | solution.py:78
  27.5 1.6 %collective-permute-start.1 = (f16[32,2176]{1,0:T(8,128)(2,1)S(1)}, f16[32,2176]{1,0:T(8,128)(2,1)S(1)}, u32[]{:S(2)}, u32[]{:S(2)}) collective-permute-start(f16[32,2176]{1,0:T(8,128)(2,1)S(1)} %convert_element_type.68), channel_id=1, source_target_pairs={{0,2},{1,3},{2,0},{3,1},{4,6},{5,7},{6,4},{7,5},{8,10},{9,11},{10,... | collective-permute-start | bytes 417800 | tf_op jit(solution)/shard_map/ppermute | solution.py:305
  29.5 3.8 %collective-permute-done.2 = f16[32,2176]{1,0:T(8,128)(2,1)S(1)} collective-permute-done((f16[32,2176]{1,0:T(8,128)(2,1)S(1)}, f16[32,2176]{1,0:T(8,128)(2,1)S(1)}, u32[]{:S(2)}, u32[]{:S(2)}) %collective-permute-start.2) | collective-permute-done | bytes 139296 | tf_op jit(solution)/shard_map/ppermute | solution.py:305
  33.4 3.0 %collective-permute-done.1 = f16[32,2176]{1,0:T(8,128)(2,1)S(1)} collective-permute-done((f16[32,2176]{1,0:T(8,128)(2,1)S(1)}, f16[32,2176]{1,0:T(8,128)(2,1)S(1)}, u32[]{:S(2)}, u32[]{:S(2)}) %collective-permute-start.1) | collective-permute-done | bytes 139296 | tf_op jit(solution)/shard_map/ppermute | solution.py:305
  36.5 5.2 %copy-done = f32[2,28,4,128,128]{4,3,2,1,0:T(8,128)S(1)} copy-done((f32[2,28,4,128,128]{4,3,2,1,0:T(8,128)S(1)}, f32[2,28,4,128,128]{4,3,2,1,0:T(8,128)}, u32[]{:S(2)}) %copy-start) | copy-done | bytes 14680088
  41.7 5.4 %cell.2 = (bf16[32,512]{1,0:T(8,128)(2,1)S(1)}, f32[2,28,4,128]{3,2,1,0:T(4,128)}, f32[2,28,4]{2,1,0:T(8,128)S(1)}, f32[4,32,128]{2,1,0:T(8,128)S(1)}, f32[4,32,...) custom-call(f32[32,2176]{1,0:T(8,128)S(1)} %get-tuple-element.24.refs_0_, f32[32,2176]{1,0:T(8,128)S(1)} %convert_element_type.67.refs_1_, ...), custom_call_target="tpu_custom_call" | custom-call | flops 7340032 | bytes 7340032 | tf_op jit(solution)/shard_map/cell/pallas_call | solution.py:198
  47.2 1.7 %collective-permute-start.4 = (bf16[32,512]{1,0:T(8,128)(2,1)S(1)}, bf16[32,512]{1,0:T(8,128)(2,1)S(1)}, u32[]{:S(2)}, u32[]{:S(2)}) collective-permute-start(bf16[32,512]{1,0:T(8,128)(2,1)S(1)} %get-tuple-element.28.refs_0_), channel_id=1, source_target_pairs={{0,2},{1,3},{2,0},{3,1},{4,6},{5,7},{6,4},{7,5},{8,10},{9,11},{10,... | collective-permute-start | bytes 98312 | tf_op jit(solution)/shard_map/ppermute | solution.py:305
  49.1 1.6 %collective-permute-done.5.refs_3_ = bf16[32,512]{1,0:T(8,128)(2,1)S(1)} collective-permute-done((bf16[32,512]{1,0:T(8,128)(2,1)S(1)}, bf16[32,512]{1,0:T(8,128)(2,1)S(1)}, u32[]{:S(2)}, u32[]{:S(2)}) %collective-permute-start.5) | collective-permute-done | bytes 32800 | tf_op jit(solution)/shard_map/ppermute | solution.py:305
  52.5 12.1 %all_to_all.20 = f16[8,16,1024]{2,1,0:T(8,128)(2,1)S(1)} all-to-all(f16[8,16,1024]{2,1,0:T(8,128)(2,1)S(1)} %bitcast.15), channel_id=1, replica_groups=mesh['tp'=8,'dp'=4] {'tp'}, dimensions={0} | all-to-all | bytes 524288 | tf_op jit(solution)/shard_map/all_to_all | solution.py:353
  64.7 11.8 %all_to_all.21 = bf16[8,16,1024]{2,1,0:T(8,128)(2,1)S(1)} all-to-all(bf16[8,16,1024]{2,1,0:T(8,128)(2,1)S(1)} %broadcast_in_dim.8), channel_id=1, replica_groups=mesh['tp'=8,'dp'=4] {'tp'}, dimensions={0} | all-to-all | bytes 524288 | tf_op jit(solution)/shard_map/all_to_all | solution.py:333
  76.5 1.6 %copy-done.9 = bf16[2,1024,512]{2,1,0:T(8,128)(2,1)S(1)} copy-done((bf16[2,1024,512]{2,1,0:T(8,128)(2,1)S(1)}, bf16[2,1024,512]{2,1,0:T(8,128)(2,1)}, u32[]{:S(2)}) %copy-start.9) | copy-done | bytes 2097176
  80.2 3.0 %project.3 = (f32[32,2176]{1,0:T(8,128)S(1)}, f32[32,2176]{1,0:T(8,128)S(1)}, f32[32,2176]{1,0:T(8,128)S(1)}, f32[32,2176]{1,0:T(8,128)S(1)}) custom-call(s32[2]{0:T(128)S(1)} %pad_add_fusion.meta, bf16[128,1024]{1,0:T(8,128)(2,1)S(1)} %bitcast.12, bf16[2,1024,512]{2,1,0:T(8,128)(2,1)S(1)} %copy-done.3, bf16[2,1024,512]{2,1,0:T(8,128)(2,1)S(1)} %copy-done.5, ...), custom_call_target="tpu_custom_call" | custom-call | flops 570425344 | bytes 5242880 | tf_op jit(solution)/shard_map/project/pallas_call | solution.py:78
  85.2 4.0 %collective-permute-done.8 = f16[32,2176]{1,0:T(8,128)(2,1)S(1)} collective-permute-done((f16[32,2176]{1,0:T(8,128)(2,1)S(1)}, f16[32,2176]{1,0:T(8,128)(2,1)S(1)}, u32[]{:S(2)}, u32[]{:S(2)}) %collective-permute-start.8) | collective-permute-done | bytes 139296 | tf_op jit(solution)/shard_map/ppermute | solution.py:305
  89.3 2.1 %collective-permute-done.7 = f16[32,2176]{1,0:T(8,128)(2,1)S(1)} collective-permute-done((f16[32,2176]{1,0:T(8,128)(2,1)S(1)}, f16[32,2176]{1,0:T(8,128)(2,1)S(1)}, u32[]{:S(2)}, u32[]{:S(2)}) %collective-permute-start.7) | collective-permute-done | bytes 139296 | tf_op jit(solution)/shard_map/ppermute | solution.py:305
  91.5 5.4 %cell.3 = (bf16[32,512]{1,0:T(8,128)(2,1)S(1)}, f32[2,28,4,128]{3,2,1,0:T(4,128)}, f32[2,28,4]{2,1,0:T(8,128)S(1)}, f32[4,32,128]{2,1,0:T(8,128)S(1)}, f32[4,32,...) custom-call(f32[32,2176]{1,0:T(8,128)S(1)} %get-tuple-element.29.refs_0_, ...), custom_call_target="tpu_custom_call", output_to_operand_aliasing={{1}: (9, {}), {2}: (10, {})} | custom-call | flops 7340032 | bytes 7340032 | tf_op jit(solution)/shard_map/cell/pallas_call | solution.py:198
  103.3 3.6 %all-to-all-start.3 = ((f16[8,16,1024]{2,1,0:T(8,128)(2,1)}), f16[8,16,1024]{2,1,0:T(8,128)(2,1)S(1)}, u32[]{:S(2)}, u32[]{:S(2)}) async-start(f16[8,16,1024]{2,1,0:T(8,128)(2,1)} %bitcast.7), calls=%async_computation.3 | async-start | bytes 524288 | tf_op jit(solution)/shard_map/all_to_all | solution.py:353
  107.0 5.2 %copy-done.1 = f32[2,28,4,128,128]{4,3,2,1,0:T(8,128)S(1)} copy-done((f32[2,28,4,128,128]{4,3,2,1,0:T(8,128)S(1)}, f32[2,28,4,128,128]{4,3,2,1,0:T(8,128)}, u32[]{:S(2)}) %copy-start.1) | copy-done | bytes 14680088
  112.1 4.9 %update.2.rest_0_ = f32[2,28,4,128,128]{4,3,2,1,0:T(8,128)} custom-call(f32[4,32,128]{2,1,0:T(8,128)S(1)} %copy-done.18, f32[4,32,128]{2,1,0:T(8,128)S(1)} %copy-done.20, f32[4,32,128]{2,1,0:T(8,128)S(1)} %copy-done.22, f32[2,28,4,128,128]{4,3,2,1,0:T(8,128)S(1)} %copy-done.1), custom_call_target="tpu_custom_call" | custom-call | flops 7340032 | bytes 14680064 | tf_op jit(solution)/shard_map/update/pallas_call | solution.py:253
  117.7 5.2 %copy-done.2 = f32[2,28,4,128,128]{4,3,2,1,0:T(8,128)S(1)} copy-done((f32[2,28,4,128,128]{4,3,2,1,0:T(8,128)S(1)}, f32[2,28,4,128,128]{4,3,2,1,0:T(8,128)}, u32[]{:S(2)}) %copy-start.2) | copy-done | bytes 14680088
  122.9 4.9 %update.3 = f32[2,28,4,128,128]{4,3,2,1,0:T(8,128)} custom-call(f32[4,32,128]{2,1,0:T(8,128)S(1)} %get-tuple-element.36.kw, f32[4,32,128]{2,1,0:T(8,128)S(1)} %get-tuple-element.37.v, f32[4,32,128]{2,1,0:T(8,128)S(1)} %get-tuple-element.38.dec, f32[2,28,4,128,128]{4,3,2,1,0:T(8,128)S(1)} %copy-done.2, ...), custom_call_target="tpu_custom_call", output_to_operand_aliasing={{}: (4, {})} | custom-call | flops 7340032 | bytes 14680064 | tf_op jit(solution)/shard_map/update/pallas_call | solution.py:253
  (101 shorter events, 21.9 us)
Async XLA Ops:
  0.6 17.9 %copy-start.3 = (bf16[2,1024,512]{2,1,0:T(8,128)(2,1)S(1)}, bf16[2,1024,512]{2,1,0:T(8,128)(2,1)}, u32[]{:S(2)}) copy-start(bf16[2,1024,512]{2,1,0:T(8,128)(2,1)} %wq.3) | copy-start | bytes 6291460
  2.3 16.2 %all-to-all-start = ((bf16[8,16,1024]{2,1,0:T(8,128)(2,1)}), bf16[8,16,1024]{2,1,0:T(8,128)(2,1)S(1)}, u32[]{:S(2)}, u32[]{:S(2)}) async-start(bf16[8,16,1024]{2,1,0:T(8,128)(2,1)} %broadcast_in_dim.6), calls=%async_computation | async-start | bytes 524288 | tf_op jit(solution)/shard_map/all_to_all | solution.py:333
  10.8 16.5 %copy-start.12 = (bf16[2,1024,32]{2,1,0:T(8,128)(2,1)}, bf16[2,1024,32]{2,1,0:T(8,128)(2,1)S(1)}, u32[]{:S(2)}) copy-start(bf16[2,1024,32]{2,1,0:T(8,128)(2,1)S(1)} %copy.20.wi) | copy-start | bytes 393220
  27.4 6.0 %collective-permute-start.2 = (f16[32,2176]{1,0:T(8,128)(2,1)S(1)}, f16[32,2176]{1,0:T(8,128)(2,1)S(1)}, u32[]{:S(2)}, u32[]{:S(2)}) collective-permute-start(f16[32,2176]{1,0:T(8,128)(2,1)S(1)} %convert_element_type.70), channel_id=1, source_target_pairs={{0,3},{1,2},{2,1},{3,0},{4,7},{5,6},{6,5},{7,4},{8,11},{9,10},{10,... | collective-permute-start | bytes 417800 | tf_op jit(solution)/shard_map/ppermute | solution.py:305
  27.5 8.9 %collective-permute-start.1 = (f16[32,2176]{1,0:T(8,128)(2,1)S(1)}, f16[32,2176]{1,0:T(8,128)(2,1)S(1)}, u32[]{:S(2)}, u32[]{:S(2)}) collective-permute-start(f16[32,2176]{1,0:T(8,128)(2,1)S(1)} %convert_element_type.68), channel_id=1, source_target_pairs={{0,2},{1,3},{2,0},{3,1},{4,6},{5,7},{6,4},{7,5},{8,10},{9,11},{10,... | collective-permute-start | bytes 417800 | tf_op jit(solution)/shard_map/ppermute | solution.py:305
  29.1 7.4 %collective-permute-start = (f16[32,2176]{1,0:T(8,128)(2,1)S(1)}, f16[32,2176]{1,0:T(8,128)(2,1)S(1)}, u32[]{:S(2)}, u32[]{:S(2)}) collective-permute-start(f16[32,2176]{1,0:T(8,128)(2,1)S(1)} %convert_element_type.66), channel_id=1, source_target_pairs={{0,1},{1,0},{2,3},{3,2},{4,5},{5,4},{6,7},{7,6},{8,9},{9,8},{10,11... | collective-permute-start | bytes 417800 | tf_op jit(solution)/shard_map/ppermute | solution.py:305
  41.7 49.8 %slice-start = ((s8[14680064]{0:T(1024)(128)(4,1)}), s8[4194304]{0:T(1024)(128)(4,1)S(1)}, s32[]{:S(2)}) async-start(s8[14680064]{0:T(1024)(128)(4,1)} %bitcast.9), calls=%async_computation.4 | async-start | bytes 8388608
  41.7 49.8 %slice-start.1 = ((s8[14680064]{0:T(1024)(128)(4,1)}), s8[4194304]{0:T(1024)(128)(4,1)S(1)}, s32[]{:S(2)}) async-start(s8[14680064]{0:T(1024)(128)(4,1)} %bitcast.9), calls=%async_computation.5 | async-start | bytes 8388608
  47.1 17.5 %copy-start.17 = (f32[4,32,128]{2,1,0:T(8,128)}, f32[4,32,128]{2,1,0:T(8,128)S(1)}, u32[]{:S(2)}) copy-start(f32[4,32,128]{2,1,0:T(8,128)S(1)} %get-tuple-element.39.kw) | copy-start | bytes 196612
  47.1 17.5 %copy-start.19 = (f32[4,32,128]{2,1,0:T(8,128)}, f32[4,32,128]{2,1,0:T(8,128)S(1)}, u32[]{:S(2)}) copy-start(f32[4,32,128]{2,1,0:T(8,128)S(1)} %get-tuple-element.40.v) | copy-start | bytes 196612
  47.1 17.5 %copy-start.21 = (f32[4,32,128]{2,1,0:T(8,128)}, f32[4,32,128]{2,1,0:T(8,128)S(1)}, u32[]{:S(2)}) copy-start(f32[4,32,128]{2,1,0:T(8,128)S(1)} %get-tuple-element.41.dec) | copy-start | bytes 196612
  47.1 29.4 %copy-start.5 = (bf16[2,1024,512]{2,1,0:T(8,128)(2,1)S(1)}, bf16[2,1024,512]{2,1,0:T(8,128)(2,1)}, u32[]{:S(2)}) copy-start(bf16[2,1024,512]{2,1,0:T(8,128)(2,1)} %wk.3) | copy-start | bytes 6291460
  47.1 29.4 %copy-start.7 = (bf16[2,1024,512]{2,1,0:T(8,128)(2,1)S(1)}, bf16[2,1024,512]{2,1,0:T(8,128)(2,1)}, u32[]{:S(2)}) copy-start(bf16[2,1024,512]{2,1,0:T(8,128)(2,1)} %wv.3) | copy-start | bytes 6291460
  47.1 44.4 %slice-start.2 = ((s8[14680064]{0:T(1024)(128)(4,1)}), s8[4194304]{0:T(1024)(128)(4,1)S(1)}, s32[]{:S(2)}) async-start(s8[14680064]{0:T(1024)(128)(4,1)} %bitcast.9), calls=%async_computation.6 | async-start | bytes 8388608
  47.1 3.5 %collective-permute-start.5 = (bf16[32,512]{1,0:T(8,128)(2,1)S(1)}, bf16[32,512]{1,0:T(8,128)(2,1)S(1)}, u32[]{:S(2)}, u32[]{:S(2)}) collective-permute-start(bf16[32,512]{1,0:T(8,128)(2,1)S(1)} %get-tuple-element.28.refs_0_), channel_id=1, source_target_pairs={{0,3},{1,2},{2,1},{3,0},{4,7},{5,6},{6,5},{7,4},{8,11},{9,10},{10,... | collective-permute-start | bytes 98312 | tf_op jit(solution)/shard_map/ppermute | solution.py:305
  47.2 4.4 %collective-permute-start.4 = (bf16[32,512]{1,0:T(8,128)(2,1)S(1)}, bf16[32,512]{1,0:T(8,128)(2,1)S(1)}, u32[]{:S(2)}, u32[]{:S(2)}) collective-permute-start(bf16[32,512]{1,0:T(8,128)(2,1)S(1)} %get-tuple-element.28.refs_0_), channel_id=1, source_target_pairs={{0,2},{1,3},{2,0},{3,1},{4,6},{5,7},{6,4},{7,5},{8,10},{9,11},{10,... | collective-permute-start | bytes 98312 | tf_op jit(solution)/shard_map/ppermute | solution.py:305
  48.9 2.7 %collective-permute-start.3 = (bf16[32,512]{1,0:T(8,128)(2,1)S(1)}, bf16[32,512]{1,0:T(8,128)(2,1)S(1)}, u32[]{:S(2)}, u32[]{:S(2)}) collective-permute-start(bf16[32,512]{1,0:T(8,128)(2,1)S(1)} %get-tuple-element.28.refs_0_), channel_id=1, source_target_pairs={{0,1},{1,0},{2,3},{3,2},{4,5},{5,4},{6,7},{7,6},{8,9},{9,8},{10,11... | collective-permute-start | bytes 98312 | tf_op jit(solution)/shard_map/ppermute | solution.py:305
  83.2 6.0 %collective-permute-start.8 = (f16[32,2176]{1,0:T(8,128)(2,1)S(1)}, f16[32,2176]{1,0:T(8,128)(2,1)S(1)}, u32[]{:S(2)}, u32[]{:S(2)}) collective-permute-start(f16[32,2176]{1,0:T(8,128)(2,1)S(1)} %convert_element_type.80), channel_id=1, source_target_pairs={{0,3},{1,2},{2,1},{3,0},{4,7},{5,6},{6,5},{7,4},{8,11},{9,10},{10,... | collective-permute-start | bytes 417800 | tf_op jit(solution)/shard_map/ppermute | solution.py:305
  83.3 8.1 %collective-permute-start.7 = (f16[32,2176]{1,0:T(8,128)(2,1)S(1)}, f16[32,2176]{1,0:T(8,128)(2,1)S(1)}, u32[]{:S(2)}, u32[]{:S(2)}) collective-permute-start(f16[32,2176]{1,0:T(8,128)(2,1)S(1)} %convert_element_type.78), channel_id=1, source_target_pairs={{0,2},{1,3},{2,0},{3,1},{4,6},{5,7},{6,4},{7,5},{8,10},{9,11},{10,... | collective-permute-start | bytes 417800 | tf_op jit(solution)/shard_map/ppermute | solution.py:305
  84.4 7.0 %collective-permute-start.6 = (f16[32,2176]{1,0:T(8,128)(2,1)S(1)}, f16[32,2176]{1,0:T(8,128)(2,1)S(1)}, u32[]{:S(2)}, u32[]{:S(2)}) collective-permute-start(f16[32,2176]{1,0:T(8,128)(2,1)S(1)} %convert_element_type.76), channel_id=1, source_target_pairs={{0,1},{1,0},{2,3},{3,2},{4,5},{5,4},{6,7},{7,6},{8,9},{9,8},{10,11... | collective-permute-start | bytes 417800 | tf_op jit(solution)/shard_map/ppermute | solution.py:305
  97.0 3.3 %collective-permute-start.11 = (bf16[32,512]{1,0:T(8,128)(2,1)S(1)}, bf16[32,512]{1,0:T(8,128)(2,1)S(1)}, u32[]{:S(2)}, u32[]{:S(2)}) collective-permute-start(bf16[32,512]{1,0:T(8,128)(2,1)S(1)} %get-tuple-element.35.refs_0_), channel_id=1, source_target_pairs={{0,3},{1,2},{2,1},{3,0},{4,7},{5,6},{6,5},{7,4},{8,11},{9,10},{10,... | collective-permute-start | bytes 98312 | tf_op jit(solution)/shard_map/ppermute | solution.py:305
  97.8 3.9 %collective-permute-start.10 = (bf16[32,512]{1,0:T(8,128)(2,1)S(1)}, bf16[32,512]{1,0:T(8,128)(2,1)S(1)}, u32[]{:S(2)}, u32[]{:S(2)}) collective-permute-start(bf16[32,512]{1,0:T(8,128)(2,1)S(1)} %get-tuple-element.35.refs_0_), channel_id=1, source_target_pairs={{0,2},{1,3},{2,0},{3,1},{4,6},{5,7},{6,4},{7,5},{8,10},{9,11},{10,... | collective-permute-start | bytes 98312 | tf_op jit(solution)/shard_map/ppermute | solution.py:305
  98.8 2.9 %collective-permute-start.9 = (bf16[32,512]{1,0:T(8,128)(2,1)S(1)}, bf16[32,512]{1,0:T(8,128)(2,1)S(1)}, u32[]{:S(2)}, u32[]{:S(2)}) collective-permute-start(bf16[32,512]{1,0:T(8,128)(2,1)S(1)} %get-tuple-element.35.refs_0_), channel_id=1, source_target_pairs={{0,1},{1,0},{2,3},{3,2},{4,5},{5,4},{6,7},{7,6},{8,9},{9,8},{10,11... | collective-permute-start | bytes 98312 | tf_op jit(solution)/shard_map/ppermute | solution.py:305
  103.3 24.5 %all-to-all-start.3 = ((f16[8,16,1024]{2,1,0:T(8,128)(2,1)}), f16[8,16,1024]{2,1,0:T(8,128)(2,1)S(1)}, u32[]{:S(2)}, u32[]{:S(2)}) async-start(f16[8,16,1024]{2,1,0:T(8,128)(2,1)} %bitcast.7), calls=%async_computation.3 | async-start | bytes 524288 | tf_op jit(solution)/shard_map/all_to_all | solution.py:353
  (20 other events, 119.0 us)

commit v2 on v1

v2 whole, which is shorter than its diff:
```python
import functools

import jax
import jax.numpy as jnp
from jax import lax
from jax.experimental import pallas as pl
from jax.experimental.pallas import tpu as pltpu
from jax.sharding import PartitionSpec as P

norm_eps = 1e-06
head_eps = 1e-05
ROWS = 32
PAD = 16
LANES = 128
UP = 12.0
TINY = 1e-30
OUT_UP = 16.0
F32 = jnp.float32
BF16 = jnp.bfloat16


def in_hbm(x):
    return pltpu.with_memory_space_constraint(x, pltpu.HBM)


def in_vmem(x):
    return pltpu.with_memory_space_constraint(x, pltpu.VMEM)


def lane_roll(x, amount):
    return pltpu.roll(x, amount % x.shape[-1], 1)


def fetch_kernel(steps, count, *refs):
    sources, targets, sems = refs[:count], refs[-1 - steps[1] : -1], refs[-1]
    copies = []
    for source, part, target, place in steps[0]:
        from_ref = sources[source] if part is None else sources[source].at[part]
        to_ref = targets[target] if place is None else targets[target].at[place]
        copies.append(pltpu.make_async_copy(from_ref, to_ref, sems.at[len(copies)]))
    for copy in copies:
        copy.start()
    if steps[2]:
        ones = targets[-1]
        for block in range(ones.shape[1] // LANES):
            row = lax.broadcasted_iota(jnp.int32, (LANES, LANES), 0)
            here = (row % ROWS == block) & (row < 3 * ROWS)
            ones[:, block * LANES : (block + 1) * LANES] = jnp.where(here, 1.0, 0.0).astype(BF16)
    for copy in copies:
        copy.wait()


def fetch(arrays, steps, shapes, with_ones=False, after=()):
    shapes = list(shapes)
    if with_ones:
        shapes.append(((LANES, ROWS * LANES), BF16))
    total = sum(a.size * a.dtype.itemsize for a in arrays)
    return pl.pallas_call(
        functools.partial(fetch_kernel, (steps, len(shapes), with_ones), len(arrays)),
        in_specs=[pl.BlockSpec(memory_space=pltpu.HBM)] * len(arrays)
        + [pl.BlockSpec(memory_space=pl.ANY)] * len(after),
        out_specs=[pl.BlockSpec(memory_space=pltpu.VMEM)] * len(shapes),
        out_shape=[pltpu.VMEM(shape, dtype) for shape, dtype in shapes],
        scratch_shapes=[pltpu.SemaphoreType.DMA((len(steps),))],
        compiler_params=pltpu.CompilerParams(vmem_limit_bytes=8 << 20),
        cost_estimate=pl.CostEstimate(flops=total, bytes_accessed=total, transcendentals=0),
        name="fetch",
    )(*map(in_hbm, arrays), *after)


def begin_kernel(tokens, *refs):
    count = (len(refs) - 2) // 2
    sources, (copied, *targets), sems = refs[:count], refs[count:-1], refs[-1]
    moves = [(tokens, copied.at[i]) for i in range(copied.shape[0])]
    moves += [(source.at[:1], target) for source, target in zip(sources, targets)]
    copies = [
        pltpu.make_async_copy(source, target, sems.at[i]) for i, (source, target) in enumerate(moves)
    ]
    for copy in copies:
        copy.start()
    for copy in copies:
        copy.wait()


def begin(tokens, weights, copies):
    shapes = [((copies,) + tokens.shape, BF16)] + [((1,) + w.shape[1:], BF16) for w in weights]
    whole = pl.BlockSpec(memory_space=pltpu.VMEM)
    return pl.pallas_call(
        begin_kernel,
        in_specs=[pl.BlockSpec(memory_space=pltpu.HBM)] * (1 + len(weights)),
        out_specs=[whole] * len(shapes),
        out_shape=[pltpu.VMEM(shape, dtype) for shape, dtype in shapes],
        scratch_shapes=[pltpu.SemaphoreType.DMA((copies + len(weights),))],
        compiler_params=pltpu.CompilerParams(vmem_limit_bytes=8 << 20),
        name="begin",
    )(*map(in_hbm, (tokens,) + weights))


def project_kernel(block, heads_all, meta, x, wq, wk, wv, wo, wi, wf, own, *rest):
    sends, (x_rel, gates) = rest[:-2], rest[-2:]
    slots = len(sends) + 1
    rows = x_rel.shape[0] // slots
    me = meta[0]
    first_head = meta[1]
    pairs, real = rows // PAD, x.shape[1]
    if real < PAD:
        x_rel[...] = jnp.zeros(x_rel.shape, BF16)
    for slot in range(slots):
        for i in range(pairs):
            at = slot * rows + i * PAD
            x_rel[at : at + real, :] = x[(me ^ slot) * pairs + i]
    xs = x_rel[...]
    cols = wq.shape[2]

    wide = xs.astype(F32)
    squares = jnp.sum(wide * wide, axis=1, keepdims=True)
    power = jnp.floor(0.5 * jnp.log2(squares + TINY))
    scale = jnp.exp2(UP - power)

    def emit(value, offset):
        width = value.shape[1]
        for slot, send in enumerate((own,) + tuple(sends)):
            send[:, offset : offset + width] = value[slot * rows : (slot + 1) * rows]

    for index, weight in enumerate((wq, wk, wv, wo)):
        emit(jnp.dot(xs, weight[block], preferred_element_type=F32) * scale, index * cols)
    gates[...] = jnp.zeros(gates.shape, F32)
    for index, weight in enumerate((wi, wf)):
        value = lax.dot_general(xs, weight[block], (((1,), (1,)), ((), ())), preferred_element_type=F32)
        gates[:, index * heads_all : (index + 1) * heads_all] = value
    lane = lax.broadcasted_iota(jnp.int32, gates.shape, 1)
    mine = pltpu.roll(gates[...], (LANES - first_head) % LANES, 1)
    mine = mine * scale
    mine = jnp.where(lane == heads_all - 1, squares * jnp.exp2(-2.0 * power), mine)
    mine = jnp.where(lane == heads_all - 2, power, mine)
    low = mine - mine.astype(BF16).astype(F32)
    emit(jnp.where(lane < LANES // 2, mine, pltpu.roll(low, LANES // 2, 1)), 4 * cols)


def project(block, meta, x, weights, slots):
    all_rows, features = x.shape[0] * PAD, x.shape[2]
    rows = all_rows // slots
    heads_all = weights[-1].shape[1]
    width = 4 * weights[0].shape[2] + LANES
    whole = pl.BlockSpec(memory_space=pltpu.VMEM)
    return pl.pallas_call(
        functools.partial(project_kernel, block, heads_all),
        in_specs=[pl.BlockSpec(memory_space=pltpu.SMEM)] + [whole] * 7,
        out_specs=[whole] * slots,
        out_shape=[jax.ShapeDtypeStruct((rows, width), F32)] * slots,
        scratch_shapes=[pltpu.VMEM((all_rows, features), BF16), pltpu.VMEM((all_rows, LANES), F32)],
        compiler_params=pltpu.CompilerParams(vmem_limit_bytes=8 << 20),
        cost_estimate=pl.CostEstimate(
            flops=2 * all_rows * features * width, bytes_accessed=1 << 20, transcendentals=0
        ),
        name="project",
    )(meta, x, *map(in_vmem, weights))


def spread(pairs, real):
    return [(slice(i * PAD, i * PAD + real), slice(i * real, (i + 1) * real)) for i in range(pairs)]


def twos(moves):
    runs = []
    for padded, plain in moves:
        length = plain.stop - plain.start
        for j in range(0, length, 2):
            runs.append((padded.start + j, plain.start + j, min(2, length - j)))
    return runs


def pieces(x):
    high = x.astype(BF16).astype(F32)
    return high, x - high


def columns(*parts):
    parts = list(parts)
    rest = LANES - sum(part.shape[0] for part in parts)
    if rest:
        parts.append(jnp.zeros((rest, LANES), F32))
    return jnp.concatenate(parts, axis=0).T.astype(BF16)


def cell_kernel(block, features, heads_all, peers, before, *refs):
    own = refs[0]
    parts = refs[1 : 1 + peers]
    bias, gain, norm, maxval, matrix, ones = refs[1 + peers : 7 + peers]
    earlier = refs[7 + peers : 7 + peers + 2 * before]
    (hidden, norm_out, max_out, kw_out, v_out, dec_out, mp_s, part_s, wide_s, tall_s) = refs[-10:]
    heads = matrix.shape[1]
    rows, real = own.shape[0], matrix.shape[0]
    pairs = rows // PAD
    moves = spread(pairs, real // pairs)
    cols = heads * LANES

    for i in range(before):
        norm_out[i] = earlier[2 * i][0]
        max_out[i] = earlier[2 * i + 1][0]
    norm_out, max_out = norm_out.at[before], max_out.at[before]

    scales, packed, squares = [], 0.0, 0.0
    for part in (own,) + tuple(parts):
        tile = part[:, 4 * cols :]
        tile = tile + lane_roll(tile, LANES // 2)
        power = tile[:, heads_all - 2 : heads_all - 1]
        scales.append(jnp.exp2(power - UP))
        packed = packed + tile * scales[-1]
        squares = squares + tile[:, heads_all - 1 : heads_all] * jnp.exp2(2.0 * power)

    def total(start, width):
        value = 0.0
        for part, scale in zip((own,) + tuple(parts), scales):
            value = value + part[:, start : start + width] * scale
        return value

    inv = lax.rsqrt(squares / features + norm_eps)
    log_in = packed[:, :heads] * inv
    raw = packed[:, heads_all : heads_all + heads] * inv + bias[block : block + 1, :]
    log_forget = jnp.minimum(raw, 0.0) - jnp.log1p(jnp.exp(-jnp.abs(raw)))
    mp_s[...] = jnp.zeros(mp_s.shape, F32)
    tall_s[...] = jnp.zeros(tall_s.shape, F32)
    wide_s[...] = jnp.zeros(wide_s.shape, F32)
    wide_s[:heads, :real] = maxval[block]
    tall = wide_s[...].T
    for padded, plain in moves:
        mp_s[padded, :] = tall[plain, :heads]
    carried = log_forget + mp_s[...]
    new_max = jnp.maximum(carried, log_in)
    decays = jnp.exp(carried - new_max)
    weight_in = jnp.exp(log_in - new_max)
    for padded, plain in moves:
        tall_s[plain, :heads] = new_max[padded]
    max_out[...] = tall_s[...].T[:heads, :real]
    part_s[...] = jnp.zeros(part_s.shape, F32)
    for h in range(heads):
        at = h * LANES
        q = total(at, LANES) * inv
        high, rest = pieces(q)
        middle, low = pieces(rest)
        q_t = columns(high, middle, low)
        for row, seq, count in twos(moves):
            spread_q = jnp.dot(
                q_t, ones[:, row * LANES : (row + count) * LANES], preferred_element_type=F32
            )
            for i in range(count):
                product = matrix[seq + i, h] * spread_q[:, i * LANES : (i + 1) * LANES]
                part_s[h, (row + i) * 8 : (row + i) * 8 + 8, :] = jnp.sum(
                    product.reshape(LANES // 8, 8, LANES), axis=0
                )
        v = total(2 * cols + at, LANES) * inv
        v_out[h] = v
        dec = jnp.broadcast_to(decays[:, h : h + 1], (rows, LANES))
        dec_out[h] = dec
        kw = total(cols + at, LANES) * (inv * LANES ** (-0.5)) * weight_in[:, h : h + 1]
        kw_out[h] = kw
        for padded, plain in moves:
            nn = dec[padded] * norm[block, plain, h, :] + kw[padded]
            norm_out[plain, h, :] = nn
            mp_s[padded, h : h + 1] = jnp.sum(q[padded] * nn, axis=1, keepdims=True)
        denominator = jnp.maximum(jnp.abs(mp_s[:, h : h + 1]), 1.0)
        mixed = part_s[h, pl.ds(0, rows, stride=8), :]
        for j in range(1, 8):
            mixed = mixed + part_s[h, pl.ds(j, rows, stride=8), :]
        scores = jnp.sum(q * kw, axis=1, keepdims=True)
        readout = (dec * mixed + scores * v) / denominator
        average = jnp.mean(readout, axis=1, keepdims=True)
        centred = readout - average
        variance = jnp.mean(centred * centred, axis=1, keepdims=True)
        normed = centred * lax.rsqrt(variance + head_eps) * gain[block, h : h + 1, :]
        gate = jax.nn.sigmoid(total(3 * cols + at, LANES) * inv)
        hidden[:, at : at + LANES] = (normed * gate).astype(BF16)


def cell(block, own, parts, bias, gain, norm, maxval, matrix, ones, heads_all, features, earlier, last, after):
    rows = own.shape[0]
    real, heads = matrix.shape[:2]
    whole = pl.BlockSpec(memory_space=pltpu.VMEM)
    gates = jax.ShapeDtypeStruct((heads, rows, LANES), F32)
    blocks = block + 1 if last else 1
    earlier = list(earlier) if last else []
    return pl.pallas_call(
        functools.partial(cell_kernel, block, features, heads_all, len(parts), len(earlier) // 2),
        in_specs=[whole] * (7 + len(parts) + len(earlier)) + [pl.BlockSpec(memory_space=pl.ANY)] * len(after),
        out_specs=[whole] * 6,
        out_shape=[
            jax.ShapeDtypeStruct((rows, heads * LANES), BF16),
            jax.ShapeDtypeStruct((blocks,) + norm.shape[1:], F32),
            jax.ShapeDtypeStruct((blocks,) + maxval.shape[1:], F32),
            gates,
            gates,
            gates,
        ],
        scratch_shapes=[
            pltpu.VMEM((rows, heads), F32),
            pltpu.VMEM((heads, rows * 8, LANES), F32),
            pltpu.VMEM((8, LANES), F32),
            pltpu.VMEM((LANES, 8), F32),
        ],
        compiler_params=pltpu.CompilerParams(vmem_limit_bytes=12 << 20),
        cost_estimate=pl.CostEstimate(
            flops=4 * real * heads * LANES * LANES, bytes_accessed=1 << 20, transcendentals=0
        ),
        name="cell",
    )(own, *parts, bias, gain, norm, maxval, in_vmem(matrix), in_vmem(ones), *earlier, *after)


def update_kernel(block, kw, v, dec, matrix, ones, *rest):
    out, buffer, sems = rest[-3:]
    real, heads = matrix.shape[:2]
    pairs = kw.shape[1] // PAD
    moves = spread(pairs, real // pairs)
    copies = []
    for h in range(heads):
        k_high, k_low = pieces(kw[h])
        k_t = columns(k_high, k_high, k_low)
        v_high, v_low = pieces(v[h])
        v_rows = jnp.concatenate([v_high, v_low, v_high, jnp.zeros_like(v_high)], axis=0).astype(BF16)
        for row, seq, count in twos(moves):
            right = jnp.concatenate(
                [ones[:, (row + i) * LANES : (row + i + 1) * LANES] * v_rows for i in range(count)], axis=1
            )
            outer = jnp.dot(k_t, right, preferred_element_type=F32)
            for i in range(count):
                decay = dec[h, row + i : row + i + 1, :]
                buffer[h, seq + i] = decay * matrix[seq + i, h] + outer[:, i * LANES : (i + 1) * LANES]
        copies.append(pltpu.make_async_copy(buffer.at[h], out.at[block, :, h], sems.at[h]))
        copies[-1].start()
    for copy in copies:
        copy.wait()


def update(block, blocks, kw, v, dec, matrix, ones, filled):
    real, heads = matrix.shape[:2]
    whole = pl.BlockSpec(memory_space=pltpu.VMEM)
    aliased = [] if filled is None else [filled]
    return pl.pallas_call(
        functools.partial(update_kernel, block),
        in_specs=[whole] * 5 + [pl.BlockSpec(memory_space=pltpu.HBM)] * len(aliased),
        out_specs=pl.BlockSpec(memory_space=pltpu.HBM),
        out_shape=pltpu.HBM((blocks,) + matrix.shape, F32),
        input_output_aliases={5: 0} if aliased else {},
        scratch_shapes=[
            pltpu.VMEM((heads, real, LANES, LANES), F32),
            pltpu.SemaphoreType.DMA((heads,)),
        ],
        compiler_params=pltpu.CompilerParams(vmem_limit_bytes=12 << 20),
        cost_estimate=pl.CostEstimate(
            flops=8 * real * heads * LANES * LANES,
            bytes_accessed=4 * real * heads * LANES * LANES,
            transcendentals=0,
        ),
        name="update",
    )(kw, v, dec, in_vmem(matrix), in_vmem(ones), *map(in_hbm, aliased))


def output_kernel(slots, meta, w, *refs):
    parts, out = refs[:slots], refs[-1]
    rows = parts[0].shape[0]
    me = meta[0]
    value = jnp.dot(
        jnp.concatenate([part[...] for part in parts], axis=0), w[0], preferred_element_type=F32
    )
    value = value * OUT_UP
    for slot in range(len(parts)):
        start = pl.multiple_of((me ^ slot) * rows, rows)
        out[pl.ds(start, rows), :] = value[slot * rows : (slot + 1) * rows]


def output(block, meta, w, parts, after):
    rows = parts[0].shape[0]
    whole = pl.BlockSpec(memory_space=pltpu.VMEM)
    return pl.pallas_call(
        functools.partial(output_kernel, len(parts)),
        in_specs=[
            pl.BlockSpec(memory_space=pltpu.SMEM),
            pl.BlockSpec((1,) + w.shape[1:], lambda i: (block, 0, 0)),
        ]
        + [whole] * len(parts)
        + [pl.BlockSpec(memory_space=pl.ANY)] * len(after),
        grid=(1,),
        out_specs=whole,
        out_shape=jax.ShapeDtypeStruct((rows * len(parts), w.shape[2]), F32),
        compiler_params=pltpu.CompilerParams(vmem_limit_bytes=12 << 20),
        cost_estimate=pl.CostEstimate(
            flops=2 * rows * len(parts) * w.shape[1] * w.shape[2], bytes_accessed=1 << 20, transcendentals=0
        ),
        name="output",
    )(meta, w, *parts, *after)


def swap(x, axis, size, bit):
    return lax.ppermute(x, axis, [(i, i ^ bit) for i in range(size)])


def on_device(
    tokens,
    w_query,
    w_key,
    w_value,
    w_outgate,
    w_ingate,
    w_forget,
    forget_bias,
    head_gain,
    w_proj,
    mem_matrix,
    mem_norm,
    mem_max,
):
    tp, dp = lax.axis_size("tp"), lax.axis_size("dp")
    real = tokens.shape[0]
    features = tokens.shape[1]
    heads = forget_bias.shape[1]
    heads_all = w_ingate.shape[2]
    assert dp & (dp - 1) == 0 and tp % dp == 0 and real <= PAD and 2 * heads_all <= LANES // 2
    assert tp // dp * PAD == ROWS and heads < heads_all - 2
    meta = jnp.stack([lax.axis_index("dp"), lax.axis_index("tp") * heads]).astype(jnp.int32)

    w_ingate, w_forget = w_ingate.swapaxes(1, 2), w_forget.swapaxes(1, 2)
    mem_max = mem_max.swapaxes(1, 2)
    blocks = w_query.shape[0]
    weights = (w_query, w_key, w_value, w_outgate, w_ingate, w_forget)
    tokens, meta = lax.optimization_barrier((tokens, meta))
    copied, *first = begin(tokens, weights, tp)
    current = lax.all_to_all(copied, "tp", 0, 0)
    earlier, matrix_out, after = [], None, ()
    for block in range(blocks):
        own, *sends = project(block, meta, current, weights if block else first, dp)
        parts = [
            swap(part.astype(jnp.float16), "dp", dp, slot).astype(F32) for slot, part in enumerate(sends, 1)
        ]
        if block == 0:
            state = mem_matrix.shape[1:]
            *matrices, ones = fetch(
                (mem_matrix,), [(0, i, i, None) for i in range(blocks)], [(state, F32)] * blocks, True, (own,)
            )
            after = tuple(matrices)
        hidden, norm_out, max_out, kw, v, dec = cell(
            block, own, parts, forget_bias, head_gain, mem_norm, mem_max, matrices[block], ones,
            heads_all, features * dp, earlier, block + 1 == blocks, after,
        )
        earlier += [norm_out, max_out]
        gathered = [hidden] + [swap(hidden, "dp", dp, slot) for slot in range(1, dp)]
        matrix_out = update(block, blocks, kw, v, dec, matrices[block], ones, matrix_out)
        after = (in_hbm(matrix_out),)
        partial = output(block, meta, w_proj, gathered, after if block + 1 == blocks else ()).reshape(tp, PAD, features)
        summed = lax.all_to_all(partial.astype(jnp.float16), "tp", 0, 0)
        summed = (jnp.sum(summed.astype(F32), axis=0) * (1.0 / OUT_UP)).astype(BF16)
        if block + 1 < blocks:
            current = lax.all_to_all(jnp.broadcast_to(summed[None], (tp,) + summed.shape), "tp", 0, 0)
    return (summed[:real], matrix_out, norm_out, max_out.swapaxes(1, 2))


def solution(mesh):
    in_specs = (
        P("tp", "dp"),
        P(None, "dp", "tp"),
        P(None, "dp", "tp"),
        P(None, "dp", "tp"),
        P(None, "dp", "tp"),
        P(None, "dp", None),
        P(None, "dp", None),
        P(None, "tp"),
        P(None, "tp", None),
        P(None, "tp", "dp"),
        P(None, "dp", "tp", None, None),
        P(None, "dp", "tp", None),
        P(None, "dp", "tp"),
    )
    out_specs = (
        P("tp", "dp"),
        P(None, "dp", "tp", None, None),
        P(None, "dp", "tp", None),
        P(None, "dp", "tp"),
    )
    return jax.shard_map(
        on_device, mesh=mesh, in_specs=in_specs, out_specs=out_specs, check_vma=False
    )
```

time: 129 us -> 93.9 us (0.73)
  local copies, waits for them, and re-layouts: 30.8 us -> 0.08 us
  blocking collectives: 23.9 us -> 52.8 us
  waiting for transfers between devices: 24.1 us -> 6.7 us
  starting transfers between devices: 18.6 us -> 7.75 us
  Pallas kernels: 28.4 us -> 24.3 us
    unnamed x64 -> x22, local copies, waits for them, and re-layouts: 29.1 us -> 0.06 us
    all_to_all x1 -> x2, blocking collectives: 11.8 us -> 27.8 us  [the longest x1 16 us: on_device(): current = lax.all_to_all(copied, 'tp', 0, 0)]
    all_to_all x1 -> x2, blocking collectives: 12.1 us -> 25 us  [on_device(): summed = lax.all_to_all(partial.astype(jnp.float16), 'tp', 0, 0)]
    ppermute x12, waiting for transfers between devices: 18.5 us -> 6.7 us  [swap(): return lax.ppermute(x, axis, [(i, i ^ bit) for i in range(size)])]
    all_to_all x2 -> x0, starting transfers between devices: 10.9 us -> none  [the longest x1 7.28 us: gather(): return lax.all_to_all(spread_rows, 'tp', 0, 0).reshape(tp * PAD, features)]
    all_to_all x2 -> x0, waiting for transfers between devices: 5.6 us -> none  [the longest x1 5.6 us: gather(): return lax.all_to_all(spread_rows, 'tp', 0, 0).reshape(tp * PAD, features)]
    pallas_call x2, Pallas kernels: 5.93 us -> 3.27 us  [project(): pl.pallas_call(functools.partial(project_kernel, block, heads_all), in_sp...]
    pallas_call x6 -> x8, Pallas kernels: 22.4 us -> 21.1 us  [the longest x2 7.48 us: update(): pl.pallas_call(functools.partial(update_kernel, block), in_specs=[whole]...]
  transfers between devices with their start and end apart: 14 -> 12, of which waited for: 9 -> 5; matrix products, arithmetic and copies ran while one was open for 3% -> 0% of each run, Pallas kernels for 8% -> 14%
where the time goes in v2:
time: 93.9 us; the launch traced here: 93.7 us
  blocking collectives  52.8 us (56%)
  Pallas kernels  24.3 us (26%)
  starting transfers between devices  7.75 us (8%)
  waiting for transfers between devices  6.7 us (7%)
  other arithmetic  1.08 us (1%)
  between operations  0.99 us (1%)
    all_to_all x2, blocking collectives, on_device(): summed = lax.all_to_all(partial.astype(jnp.float16), 'tp', 0, 0)  25 us
    all_to_all x1, blocking collectives, on_device(): current = lax.all_to_all(copied, 'tp', 0, 0)  16 us
    all_to_all x1, blocking collectives, on_device(): lax.all_to_all(jnp.broadcast_to(summed[None], (tp,) + summed.shape), 'tp'...  11.8 us
    ppermute x12, starting transfers between devices, swap(): return lax.ppermute(x, axis, [(i, i ^ bit) for i in range(size)])  7.75 us
    pallas_call x2, Pallas kernels, update(): pl.pallas_call(functools.partial(update_kernel, block), in_specs=[whole]...  7.48 us
    ppermute x12, waiting for transfers between devices, swap(): return lax.ppermute(x, axis, [(i, i ^ bit) for i in range(size)])  6.7 us
    pallas_call x1, Pallas kernels, fetch(): pl.pallas_call(functools.partial(fetch_kernel, (steps, len(shapes), with_...  5.23 us
    pallas_call x2, Pallas kernels, cell(): pl.pallas_call(functools.partial(cell_kernel, block, features, heads_all,...  4.18 us
  transfers between devices with their start and end apart: 12, of which 5 were waited for; matrix products, arithmetic and copies ran while one was open for 0% of the time, Pallas kernels for 14%

profile of v2, /device:TPU:0, one launch (start us, length us, event | category | flops | bytes accessed | tf_op | source)
XLA Modules:
  0.0 93.7 jit_solution(5638824956712919092)
XLA Ops:
  0.7 2.4 %begin.1 = (bf16[8,14,1024]{2,1,0:T(8,128)(2,1)S(1)}, bf16[1,1024,512]{2,1,0:T(8,128)(2,1)S(1)}, bf16[1,1024,512]{2,1,0:T(8,128)(2,1)S(1)}, bf16[1,1024,512]{2,1...) custom-call(bf16[14,1024]{1,0:T(8,128)(2,1)} %tokens, ...), custom_call_target="tpu_custom_call" | custom-call | tf_op jit(solution)/shard_map/begin/pallas_call | solution.py:88
  3.2 16.0 %all_to_all.20.x = bf16[8,14,1024]{2,1,0:T(8,128)(2,1)S(1)} all-to-all(bf16[8,14,1024]{2,1,0:T(8,128)(2,1)S(1)} %get-tuple-element.38), channel_id=1, replica_groups=mesh['tp'=8,'dp'=4] {'tp'}, dimensions={0} | all-to-all | bytes 458752 | tf_op jit(solution)/shard_map/all_to_all | solution.py:427
  19.2 1.6 %project.2 = (f32[32,2176]{1,0:T(8,128)S(1)}, f32[32,2176]{1,0:T(8,128)S(1)}, f32[32,2176]{1,0:T(8,128)S(1)}, f32[32,2176]{1,0:T(8,128)S(1)}) custom-call(s32[2]{0:T(128)S(1)} %pad_add_fusion.meta, bf16[8,14,1024]{2,1,0:T(8,128)(2,1)S(1)} %all_to_all.20.x, bf16[1,1024,512]{2,1,0:T(8,128)(2,1)S(1)} %get-tuple-element.39.wq, ...), custom_call_target="tpu_custom_call" | custom-call | flops 570425344 | bytes 1048576 | tf_op jit(solution)/shard_map/project/pallas_call | solution.py:146
  20.9 1.6 %collective-permute-start.1 = (f16[32,2176]{1,0:T(8,128)(2,1)S(1)}, f16[32,2176]{1,0:T(8,128)(2,1)S(1)}, u32[]{:S(2)}, u32[]{:S(2)}) collective-permute-start(f16[32,2176]{1,0:T(8,128)(2,1)S(1)} %convert_element_type.66), channel_id=1, source_target_pairs={{0,2},{1,3},{2,0},{3,1},{4,6},{5,7},{6,4},{7,5},{8,10},{9,11},{10,... | collective-permute-start | bytes 417800 | tf_op jit(solution)/shard_map/ppermute | solution.py:394
  22.9 5.2 %fetch.1 = (f32[28,4,128,128]{3,2,1,0:T(8,128)S(1)}, f32[28,4,128,128]{3,2,1,0:T(8,128)S(1)}, bf16[128,4096]{1,0:T(8,128)(2,1)S(1)}) custom-call(f32[2,28,4,128,128]{4,3,2,1,0:T(8,128)} %refs_0_.3, f32[32,2176]{1,0:T(8,128)S(1)} %get-tuple-element.45.refs_1_.refs_0_), custom_call_target="tpu_custom_call" | custom-call | flops 14680064 | bytes 14680064 | tf_op jit(solution)/shard_map/fetch/pallas_call | solution.py:58
  28.2 1.7 %collective-permute-done.1 = f16[32,2176]{1,0:T(8,128)(2,1)S(1)} collective-permute-done((f16[32,2176]{1,0:T(8,128)(2,1)S(1)}, f16[32,2176]{1,0:T(8,128)(2,1)S(1)}, u32[]{:S(2)}, u32[]{:S(2)}) %collective-permute-start.1) | collective-permute-done | bytes 139296 | tf_op jit(solution)/shard_map/ppermute | solution.py:394
  30.1 1.8 %cell.2 = (bf16[32,512]{1,0:T(8,128)(2,1)S(1)}, f32[1,28,4,128]{3,2,1,0:T(4,128)S(1)}, f32[1,4,28]{2,1,0:T(4,128)S(1)}, f32[4,32,128]{2,1,0:T(8,128)S(1)}, f32[4...) custom-call(f32[32,2176]{1,0:T(8,128)S(1)} %get-tuple-element.45.refs_1_.refs_0_, ...), custom_call_target="tpu_custom_call" | custom-call | flops 7340032 | bytes 1048576 | tf_op jit(solution)/shard_map/cell/pallas_call | solution.py:283
  31.9 1.7 %collective-permute-start.4 = (bf16[32,512]{1,0:T(8,128)(2,1)S(1)}, bf16[32,512]{1,0:T(8,128)(2,1)S(1)}, u32[]{:S(2)}, u32[]{:S(2)}) collective-permute-start(bf16[32,512]{1,0:T(8,128)(2,1)S(1)} %get-tuple-element.52.refs_0_), channel_id=1, source_target_pairs={{0,2},{1,3},{2,0},{3,1},{4,6},{5,7},{6,4},{7,5},{8,10},{9,11},{10,... | collective-permute-start | bytes 98312 | tf_op jit(solution)/shard_map/ppermute | solution.py:394
  33.8 1.6 %collective-permute-done.5.refs_3_ = bf16[32,512]{1,0:T(8,128)(2,1)S(1)} collective-permute-done((bf16[32,512]{1,0:T(8,128)(2,1)S(1)}, bf16[32,512]{1,0:T(8,128)(2,1)S(1)}, u32[]{:S(2)}, u32[]{:S(2)}) %collective-permute-start.5) | collective-permute-done | bytes 32800 | tf_op jit(solution)/shard_map/ppermute | solution.py:394
  35.4 0.9 collective-permute-done.4.refs_2_
  36.3 0.9 output.2
  37.2 12.0 %all_to_all.21 = f16[8,16,1024]{2,1,0:T(8,128)(2,1)S(1)} all-to-all(f16[8,16,1024]{2,1,0:T(8,128)(2,1)S(1)} %bitcast.14), channel_id=1, replica_groups=mesh['tp'=8,'dp'=4] {'tp'}, dimensions={0} | all-to-all | bytes 524288 | tf_op jit(solution)/shard_map/all_to_all | solution.py:449
  49.3 11.8 %all_to_all.22.x = bf16[8,16,1024]{2,1,0:T(8,128)(2,1)S(1)} all-to-all(bf16[8,16,1024]{2,1,0:T(8,128)(2,1)S(1)} %broadcast_in_dim.2), channel_id=1, replica_groups=mesh['tp'=8,'dp'=4] {'tp'}, dimensions={0} | all-to-all | bytes 524288 | tf_op jit(solution)/shard_map/all_to_all | solution.py:452
  61.2 1.6 %project.3 = (f32[32,2176]{1,0:T(8,128)S(1)}, f32[32,2176]{1,0:T(8,128)S(1)}, f32[32,2176]{1,0:T(8,128)S(1)}, f32[32,2176]{1,0:T(8,128)S(1)}) custom-call(s32[2]{0:T(128)S(1)} %pad_add_fusion.meta, bf16[8,16,1024]{2,1,0:T(8,128)(2,1)S(1)} %all_to_all.22.x, bf16[2,1024,512]{2,1,0:T(8,128)(2,1)S(1)} %copy-done.1, bf16[2,1024,512]{2,1,0:T(8,128)(2,1)S(1)} %copy-done.2, ...), custom_call_target="tpu_custom_call" | custom-call | flops 570425344 | bytes 1048576 | tf_op jit(solution)/shard_map/project/pallas_call | solution.py:146
  62.9 1.1 %collective-permute-start.7 = (f16[32,2176]{1,0:T(8,128)(2,1)S(1)}, f16[32,2176]{1,0:T(8,128)(2,1)S(1)}, u32[]{:S(2)}, u32[]{:S(2)}) collective-permute-start(f16[32,2176]{1,0:T(8,128)(2,1)S(1)} %convert_element_type.76), channel_id=1, source_target_pairs={{0,2},{1,3},{2,0},{3,1},{4,6},{5,7},{6,4},{7,5},{8,10},{9,11},{10,... | collective-permute-start | bytes 417800 | tf_op jit(solution)/shard_map/ppermute | solution.py:394
  64.1 0.8 collective-permute-start.6
  64.9 3.7 %update.2.refs_12_.rest_0_ = f32[2,28,4,128,128]{4,3,2,1,0:T(8,128)} custom-call(f32[4,32,128]{2,1,0:T(8,128)S(1)} %get-tuple-element.59.kw, f32[4,32,128]{2,1,0:T(8,128)S(1)} %get-tuple-element.60.v, f32[4,32,128]{2,1,0:T(8,128)S(1)} %get-tuple-element.61.dec, f32[28,4,128,128]{3,2,1,0:T(8,128)S(1)} %get-tuple-element.49.refs_8_.refs_10_.matrix, ...), custom_call_target="tpu_custom_call" | custom-call | flops 14680064 | bytes 7340032 | tf_op jit(solution)/shard_map/update/pallas_call | solution.py:338
  68.9 2.2 %collective-permute-done.7 = f16[32,2176]{1,0:T(8,128)(2,1)S(1)} collective-permute-done((f16[32,2176]{1,0:T(8,128)(2,1)S(1)}, f16[32,2176]{1,0:T(8,128)(2,1)S(1)}, u32[]{:S(2)}, u32[]{:S(2)}) %collective-permute-start.7) | collective-permute-done | bytes 139296 | tf_op jit(solution)/shard_map/ppermute | solution.py:394
  71.1 2.4 %cell.3 = (bf16[32,512]{1,0:T(8,128)(2,1)S(1)}, f32[2,28,4,128]{3,2,1,0:T(4,128)}, f32[2,4,28]{2,1,0:T(4,128)}, f32[4,32,128]{2,1,0:T(8,128)S(1)}, f32[4,32,128]{2,1,0:T(8,128)S(1)}, /*index=5*/f32[4,32,128]{2,1,0:T(8,128)S(1)}) custom-call(f32[32,2176]{1,0:T(8,128)S(1)} %get-tuple-element.53.refs_0_, f32[32,2176]{1,0:T(8,128)S(1)} %convert_element_type.75.refs_1_, ...), custom_call_target="tpu_custom_call" | custom-call | flops 7340032 | bytes 1048576 | tf_op jit(solution)/shard_map/cell/pallas_call | solution.py:283
  73.6 0.8 collective-permute-start.11
  74.4 1.0 %collective-permute-start.10 = (bf16[32,512]{1,0:T(8,128)(2,1)S(1)}, bf16[32,512]{1,0:T(8,128)(2,1)S(1)}, u32[]{:S(2)}, u32[]{:S(2)}) collective-permute-start(bf16[32,512]{1,0:T(8,128)(2,1)S(1)} %get-tuple-element.62.refs_0_), channel_id=1, source_target_pairs={{0,2},{1,3},{2,0},{3,1},{4,6},{5,7},{6,4},{7,5},{8,10},{9,11},{10,... | collective-permute-start | bytes 98312 | tf_op jit(solution)/shard_map/ppermute | solution.py:394
  75.4 3.7 %update.3.refs_4_ = f32[2,28,4,128,128]{4,3,2,1,0:T(8,128)} custom-call(f32[4,32,128]{2,1,0:T(8,128)S(1)} %get-tuple-element.63.kw, f32[4,32,128]{2,1,0:T(8,128)S(1)} %get-tuple-element.64.v, f32[4,32,128]{2,1,0:T(8,128)S(1)} %get-tuple-element.65.dec, ...), custom_call_target="tpu_custom_call", output_to_operand_aliasing={{}: (5, {})} | custom-call | flops 14680064 | bytes 7340032 | tf_op jit(solution)/shard_map/update/pallas_call | solution.py:338
  79.2 0.9 output.3
  80.1 12.9 %all_to_all.23 = f16[8,16,1024]{2,1,0:T(8,128)(2,1)S(1)} all-to-all(f16[8,16,1024]{2,1,0:T(8,128)(2,1)S(1)} %bitcast.15), channel_id=1, replica_groups=mesh['tp'=8,'dp'=4] {'tp'}, dimensions={0} | all-to-all | bytes 524288 | tf_op jit(solution)/shard_map/all_to_all | solution.py:449
  (56 shorter events, 2.2 us)
Async XLA Ops:
  20.9 7.3 %collective-permute-start.2 = (f16[32,2176]{1,0:T(8,128)(2,1)S(1)}, f16[32,2176]{1,0:T(8,128)(2,1)S(1)}, u32[]{:S(2)}, u32[]{:S(2)}) collective-permute-start(f16[32,2176]{1,0:T(8,128)(2,1)S(1)} %convert_element_type.68), channel_id=1, source_target_pairs={{0,3},{1,2},{2,1},{3,0},{4,7},{5,6},{6,5},{7,4},{8,11},{9,10},{10,... | collective-permute-start | bytes 417800 | tf_op jit(solution)/shard_map/ppermute | solution.py:394
  20.9 8.9 %collective-permute-start.1 = (f16[32,2176]{1,0:T(8,128)(2,1)S(1)}, f16[32,2176]{1,0:T(8,128)(2,1)S(1)}, u32[]{:S(2)}, u32[]{:S(2)}) collective-permute-start(f16[32,2176]{1,0:T(8,128)(2,1)S(1)} %convert_element_type.66), channel_id=1, source_target_pairs={{0,2},{1,3},{2,0},{3,1},{4,6},{5,7},{6,4},{7,5},{8,10},{9,11},{10,... | collective-permute-start | bytes 417800 | tf_op jit(solution)/shard_map/ppermute | solution.py:394
  22.5 7.4 %collective-permute-start = (f16[32,2176]{1,0:T(8,128)(2,1)S(1)}, f16[32,2176]{1,0:T(8,128)(2,1)S(1)}, u32[]{:S(2)}, u32[]{:S(2)}) collective-permute-start(f16[32,2176]{1,0:T(8,128)(2,1)S(1)} %convert_element_type.64), channel_id=1, source_target_pairs={{0,1},{1,0},{2,3},{3,2},{4,5},{5,4},{6,7},{7,6},{8,9},{9,8},{10,11... | collective-permute-start | bytes 417800 | tf_op jit(solution)/shard_map/ppermute | solution.py:394
  22.9 7.1 %copy-start.7 = (f32[2,28,4,128]{3,2,1,0:T(4,128)S(1)}, f32[2,28,4,128]{3,2,1,0:T(4,128)}, u32[]{:S(2)}) copy-start(f32[2,28,4,128]{3,2,1,0:T(4,128)} %refs_6_.3) | copy-start | bytes 344068
  22.9 7.1 %copy-start.8 = (f32[2,4,128]{2,1,0:T(4,128)S(1)}, f32[2,4,128]{2,1,0:T(4,128)}, u32[]{:S(2)}) copy-start(f32[2,4,128]{2,1,0:T(4,128)} %refs_5_.3) | copy-start | bytes 12292
  22.9 7.1 %copy-start.9 = (f32[2,28,4]{1,2,0:T(4,128)S(1)}, f32[2,28,4]{1,2,0:T(4,128)}, u32[]{:S(2)}) copy-start(f32[2,28,4]{1,2,0:T(4,128)} %param.25) | copy-start | bytes 2692
  22.9 7.1 %copy-start.10 = (f32[2,4]{1,0:T(2,128)S(1)}, f32[2,4]{1,0:T(2,128)}, u32[]{:S(2)}) copy-start(f32[2,4]{1,0:T(2,128)} %refs_4_.3) | copy-start | bytes 100
  30.0 6.3 %copy-start = (bf16[2,512,1024]{2,1,0:T(8,128)(2,1)S(1)}, bf16[2,512,1024]{2,1,0:T(8,128)(2,1)}, u32[]{:S(2)}) copy-start(bf16[2,512,1024]{2,1,0:T(8,128)(2,1)} %w.3) | copy-start | bytes 6291460
  30.0 31.2 %copy-start.1 = (bf16[2,1024,512]{2,1,0:T(8,128)(2,1)S(1)}, bf16[2,1024,512]{2,1,0:T(8,128)(2,1)}, u32[]{:S(2)}) copy-start(bf16[2,1024,512]{2,1,0:T(8,128)(2,1)} %wq.1) | copy-start | bytes 6291460
  30.0 31.1 %copy-start.2 = (bf16[2,1024,512]{2,1,0:T(8,128)(2,1)S(1)}, bf16[2,1024,512]{2,1,0:T(8,128)(2,1)}, u32[]{:S(2)}) copy-start(bf16[2,1024,512]{2,1,0:T(8,128)(2,1)} %wk.1) | copy-start | bytes 6291460
  30.0 31.1 %copy-start.3 = (bf16[2,1024,512]{2,1,0:T(8,128)(2,1)S(1)}, bf16[2,1024,512]{2,1,0:T(8,128)(2,1)}, u32[]{:S(2)}) copy-start(bf16[2,1024,512]{2,1,0:T(8,128)(2,1)} %wv.1) | copy-start | bytes 6291460
  30.0 31.1 %copy-start.4 = (bf16[2,1024,512]{2,1,0:T(8,128)(2,1)S(1)}, bf16[2,1024,512]{2,1,0:T(8,128)(2,1)}, u32[]{:S(2)}) copy-start(bf16[2,1024,512]{2,1,0:T(8,128)(2,1)} %wo.1) | copy-start | bytes 6291460
  30.0 31.1 %copy-start.5 = (bf16[2,1024,32]{1,2,0:T(8,128)(2,1)S(1)}, bf16[2,1024,32]{1,2,0:T(8,128)(2,1)}, u32[]{:S(2)}) copy-start(bf16[2,1024,32]{1,2,0:T(8,128)(2,1)} %param.18) | copy-start | bytes 393220
  30.1 31.1 %copy-start.6 = (bf16[2,1024,32]{1,2,0:T(8,128)(2,1)S(1)}, bf16[2,1024,32]{1,2,0:T(8,128)(2,1)}, u32[]{:S(2)}) copy-start(bf16[2,1024,32]{1,2,0:T(8,128)(2,1)} %param.19) | copy-start | bytes 393220
  31.8 3.5 %collective-permute-start.5 = (bf16[32,512]{1,0:T(8,128)(2,1)S(1)}, bf16[32,512]{1,0:T(8,128)(2,1)S(1)}, u32[]{:S(2)}, u32[]{:S(2)}) collective-permute-start(bf16[32,512]{1,0:T(8,128)(2,1)S(1)} %get-tuple-element.52.refs_0_), channel_id=1, source_target_pairs={{0,3},{1,2},{2,1},{3,0},{4,7},{5,6},{6,5},{7,4},{8,11},{9,10},{10,... | collective-permute-start | bytes 98312 | tf_op jit(solution)/shard_map/ppermute | solution.py:394
  31.9 4.4 %collective-permute-start.4 = (bf16[32,512]{1,0:T(8,128)(2,1)S(1)}, bf16[32,512]{1,0:T(8,128)(2,1)S(1)}, u32[]{:S(2)}, u32[]{:S(2)}) collective-permute-start(bf16[32,512]{1,0:T(8,128)(2,1)S(1)} %get-tuple-element.52.refs_0_), channel_id=1, source_target_pairs={{0,2},{1,3},{2,0},{3,1},{4,6},{5,7},{6,4},{7,5},{8,10},{9,11},{10,... | collective-permute-start | bytes 98312 | tf_op jit(solution)/shard_map/ppermute | solution.py:394
  33.6 2.7 %collective-permute-start.3 = (bf16[32,512]{1,0:T(8,128)(2,1)S(1)}, bf16[32,512]{1,0:T(8,128)(2,1)S(1)}, u32[]{:S(2)}, u32[]{:S(2)}) collective-permute-start(bf16[32,512]{1,0:T(8,128)(2,1)S(1)} %get-tuple-element.52.refs_0_), channel_id=1, source_target_pairs={{0,1},{1,0},{2,3},{3,2},{4,5},{5,4},{6,7},{7,6},{8,9},{9,8},{10,11... | collective-permute-start | bytes 98312 | tf_op jit(solution)/shard_map/ppermute | solution.py:394
  62.9 6.0 %collective-permute-start.8 = (f16[32,2176]{1,0:T(8,128)(2,1)S(1)}, f16[32,2176]{1,0:T(8,128)(2,1)S(1)}, u32[]{:S(2)}, u32[]{:S(2)}) collective-permute-start(f16[32,2176]{1,0:T(8,128)(2,1)S(1)} %convert_element_type.78), channel_id=1, source_target_pairs={{0,3},{1,2},{2,1},{3,0},{4,7},{5,6},{6,5},{7,4},{8,11},{9,10},{10,... | collective-permute-start | bytes 417800 | tf_op jit(solution)/shard_map/ppermute | solution.py:394
  62.9 8.1 %collective-permute-start.7 = (f16[32,2176]{1,0:T(8,128)(2,1)S(1)}, f16[32,2176]{1,0:T(8,128)(2,1)S(1)}, u32[]{:S(2)}, u32[]{:S(2)}) collective-permute-start(f16[32,2176]{1,0:T(8,128)(2,1)S(1)} %convert_element_type.76), channel_id=1, source_target_pairs={{0,2},{1,3},{2,0},{3,1},{4,6},{5,7},{6,4},{7,5},{8,10},{9,11},{10,... | collective-permute-start | bytes 417800 | tf_op jit(solution)/shard_map/ppermute | solution.py:394
  64.1 7.0 %collective-permute-start.6 = (f16[32,2176]{1,0:T(8,128)(2,1)S(1)}, f16[32,2176]{1,0:T(8,128)(2,1)S(1)}, u32[]{:S(2)}, u32[]{:S(2)}) collective-permute-start(f16[32,2176]{1,0:T(8,128)(2,1)S(1)} %convert_element_type.74), channel_id=1, source_target_pairs={{0,1},{1,0},{2,3},{3,2},{4,5},{5,4},{6,7},{7,6},{8,9},{9,8},{10,11... | collective-permute-start | bytes 417800 | tf_op jit(solution)/shard_map/ppermute | solution.py:394
  73.6 5.6 %collective-permute-start.11 = (bf16[32,512]{1,0:T(8,128)(2,1)S(1)}, bf16[32,512]{1,0:T(8,128)(2,1)S(1)}, u32[]{:S(2)}, u32[]{:S(2)}) collective-permute-start(bf16[32,512]{1,0:T(8,128)(2,1)S(1)} %get-tuple-element.62.refs_0_), channel_id=1, source_target_pairs={{0,3},{1,2},{2,1},{3,0},{4,7},{5,6},{6,5},{7,4},{8,11},{9,10},{10,... | collective-permute-start | bytes 98312 | tf_op jit(solution)/shard_map/ppermute | solution.py:394
  74.4 4.8 %collective-permute-start.10 = (bf16[32,512]{1,0:T(8,128)(2,1)S(1)}, bf16[32,512]{1,0:T(8,128)(2,1)S(1)}, u32[]{:S(2)}, u32[]{:S(2)}) collective-permute-start(bf16[32,512]{1,0:T(8,128)(2,1)S(1)} %get-tuple-element.62.refs_0_), channel_id=1, source_target_pairs={{0,2},{1,3},{2,0},{3,1},{4,6},{5,7},{6,4},{7,5},{8,10},{9,11},{10,... | collective-permute-start | bytes 98312 | tf_op jit(solution)/shard_map/ppermute | solution.py:394
  75.4 3.8 %collective-permute-start.9 = (bf16[32,512]{1,0:T(8,128)(2,1)S(1)}, bf16[32,512]{1,0:T(8,128)(2,1)S(1)}, u32[]{:S(2)}, u32[]{:S(2)}) collective-permute-start(bf16[32,512]{1,0:T(8,128)(2,1)S(1)} %get-tuple-element.62.refs_0_), channel_id=1, source_target_pairs={{0,1},{1,0},{2,3},{3,2},{4,5},{5,4},{6,7},{7,6},{8,9},{9,8},{10,11... | collective-permute-start | bytes 98312 | tf_op jit(solution)/shard_map/ppermute | solution.py:394

commit v3 on v2

--- a/solution.py
+++ b/solution.py
@@ -96,65 +96,136 @@
     )(*map(in_hbm, (tokens,) + weights))
 
 
-def project_kernel(block, heads_all, meta, x, wq, wk, wv, wo, wi, wf, own, *rest):
-    sends, (x_rel, gates) = rest[:-2], rest[-2:]
-    slots = len(sends) + 1
-    rows = x_rel.shape[0] // slots
+def first_project_kernel(block, heads_all, meta, x, wq, wk, wi, wf, keep, send, x_rel, gates):
+    rows = ROWS
+    slots = x_rel.shape[0] // rows
     me = meta[0]
     first_head = meta[1]
     pairs, real = rows // PAD, x.shape[1]
     if real < PAD:
         x_rel[...] = jnp.zeros(x_rel.shape, BF16)
-    for slot in range(slots):
+    for place, slot in enumerate(slot_order(slots)):
         for i in range(pairs):
-            at = slot * rows + i * PAD
+            at = place * rows + i * PAD
             x_rel[at : at + real, :] = x[(me ^ slot) * pairs + i]
     xs = x_rel[...]
     cols = wq.shape[2]
-
+    half = keep.shape[0]
+
+    def emit(value, offset):
+        width = value.shape[1]
+        keep[:, offset : offset + width] = value[:half]
+        send[:, offset : offset + width] = value[half:]
+
+    for index, weight in enumerate((wq, wk)):
+        emit(jnp.dot(xs, weight[block], preferred_element_type=F32), index * cols)
     wide = xs.astype(F32)
     squares = jnp.sum(wide * wide, axis=1, keepdims=True)
-    power = jnp.floor(0.5 * jnp.log2(squares + TINY))
-    scale = jnp.exp2(UP - power)
-
-    def emit(value, offset):
-        width = value.shape[1]
-        for slot, send in enumerate((own,) + tuple(sends)):
-            send[:, offset : offset + width] = value[slot * rows : (slot + 1) * rows]
-
-    for index, weight in enumerate((wq, wk, wv, wo)):
-        emit(jnp.dot(xs, weight[block], preferred_element_type=F32) * scale, index * cols)
     gates[...] = jnp.zeros(gates.shape, F32)
     for index, weight in enumerate((wi, wf)):
         value = lax.dot_general(xs, weight[block], (((1,), (1,)), ((), ())), preferred_element_type=F32)
         gates[:, index * heads_all : (index + 1) * heads_all] = value
     lane = lax.broadcasted_iota(jnp.int32, gates.shape, 1)
     mine = pltpu.roll(gates[...], (LANES - first_head) % LANES, 1)
-    mine = mine * scale
-    mine = jnp.where(lane == heads_all - 1, squares * jnp.exp2(-2.0 * power), mine)
-    mine = jnp.where(lane == heads_all - 2, power, mine)
-    low = mine - mine.astype(BF16).astype(F32)
-    emit(jnp.where(lane < LANES // 2, mine, pltpu.roll(low, LANES // 2, 1)), 4 * cols)
-
-
-def project(block, meta, x, weights, slots):
-    all_rows, features = x.shape[0] * PAD, x.shape[2]
-    rows = all_rows // slots
-    heads_all = weights[-1].shape[1]
-    width = 4 * weights[0].shape[2] + LANES
+    emit(jnp.where(lane == heads_all - 1, squares, mine), 2 * cols)
+
+
+def second_project_kernel(block, x_rel, wv, wo, keep, send):
+    xs = x_rel[...]
+    cols = wv.shape[2]
+    half = keep.shape[0]
+    for index, weight in enumerate((wv, wo)):
+        value = jnp.dot(xs, weight[block], preferred_element_type=F32)
+        keep[:, index * cols : (index + 1) * cols] = value[:half]
+        send[:, index * cols : (index + 1) * cols] = value[half:]
+
+
+def first_add_kernel(heads_all, keep, other, scale_out, *outs):
+    wide = keep.shape[1]
+    tile = keep[:, wide - LANES :] + other[:, wide - LANES :]
+    squares = tile[:, heads_all - 1 : heads_all]
+    power = jnp.floor(0.5 * jnp.log2(squares + TINY))
+    scale = jnp.exp2(UP - power)
+    scale_out[...] = jnp.broadcast_to(scale, scale_out.shape)
+    lane = lax.broadcasted_iota(jnp.int32, tile.shape, 1)
+    tile = tile * scale
+    tile = jnp.where(lane == heads_all - 1, squares * jnp.exp2(-2.0 * power), tile)
+    tile = jnp.where(lane == heads_all - 2, power, tile)
+    low = tile - tile.astype(BF16).astype(F32)
+    tile = jnp.where(lane < LANES // 2, tile, pltpu.roll(low, LANES // 2, 1))
+    for i, out in enumerate(outs):
+        at = slice(i * ROWS, (i + 1) * ROWS)
+        out[:, : wide - LANES] = (keep[at, : wide - LANES] + other[at, : wide - LANES]) * scale[at]
+        out[:, wide - LANES :] = tile[at]
+
+
+def second_add_kernel(keep, other, scale, *outs):
+    for i, out in enumerate(outs):
+        at = slice(i * ROWS, (i + 1) * ROWS)
+        out[...] = (keep[at] + other[at]) * scale[at, :1]
+
+
+def slot_order(slots):
+    return list(range(0, slots, 2)) + list(range(1, slots, 2))
+
+
+def small_call(kernel, name, shapes, args, scratch=(), scalars=0, flops=0):
     whole = pl.BlockSpec(memory_space=pltpu.VMEM)
     return pl.pallas_call(
-        functools.partial(project_kernel, block, heads_all),
-        in_specs=[pl.BlockSpec(memory_space=pltpu.SMEM)] + [whole] * 7,
-        out_specs=[whole] * slots,
-        out_shape=[jax.ShapeDtypeStruct((rows, width), F32)] * slots,
-        scratch_shapes=[pltpu.VMEM((all_rows, features), BF16), pltpu.VMEM((all_rows, LANES), F32)],
+        kernel,
+        in_specs=[pl.BlockSpec(memory_space=pltpu.SMEM)] * scalars + [whole] * (len(args) - scalars),
+        out_specs=[whole] * len(shapes),
+        out_shape=[jax.ShapeDtypeStruct(shape, dtype) for shape, dtype in shapes],
+        scratch_shapes=list(scratch),
         compiler_params=pltpu.CompilerParams(vmem_limit_bytes=8 << 20),
-        cost_estimate=pl.CostEstimate(
-            flops=2 * all_rows * features * width, bytes_accessed=1 << 20, transcendentals=0
-        ),
-        name="project",
-    )(meta, x, *map(in_vmem, weights))
+        cost_estimate=pl.CostEstimate(flops=flops, bytes_accessed=1 << 20, transcendentals=0),
+        name=name,
+    )(*args)
+
+
+def project(block, meta, x, weights, slots):
+    wq, wk, wv, wo, wi, wf = map(in_vmem, weights)
+    all_rows, features = slots * ROWS, x.shape[2]
+    half = all_rows // 2
+    cols, heads_all = wq.shape[2], wi.shape[1]
+    first, second = 2 * cols + LANES, 2 * cols
+    flops = 2 * all_rows * features * second
+    keep_a, send_a, x_rel = small_call(
+        functools.partial(first_project_kernel, block, heads_all),
+        "project_first",
+        [((half, first), F32)] * 2 + [((all_rows, features), BF16)],
+        (meta, x, wq, wk, wi, wf),
+        [pltpu.VMEM((all_rows, LANES), F32)],
+        1,
+        flops,
+    )
+    other_a = swap(send_a, "dp", slots, 1)
+    keep_b, send_b = small_call(
+        functools.partial(second_project_kernel, block),
+        "project_second",
+        [((half, second), F32)] * 2,
+        (x_rel, wv, wo),
+        flops=flops,
+    )
+    other_b = swap(send_b, "dp", slots, 1)
+    scale, *sums_a = small_call(
+        functools.partial(first_add_kernel, heads_all),
+        "add_first",
+        [((half, LANES), F32)] + [((ROWS, first), F32)] * (slots // 2),
+        (keep_a, other_a),
+        flops=1 << 20,
+    )
+    sums_b = small_call(
+        second_add_kernel, "add_second", [((ROWS, second), F32)] * (slots // 2), (keep_b, other_b, scale), flops=1 << 20
+    )
+
+    def across(sums):
+        return [sums[0]] + [
+            swap(part.astype(jnp.float16), "dp", slots, slot).astype(F32)
+            for part, slot in zip(sums[1:], range(2, slots, 2))
+        ]
+
+    return across(sums_a), across(sums_b)
 
 
 def spread(pairs, real):
@@ -184,13 +255,12 @@
 
 
 def cell_kernel(block, features, heads_all, peers, before, *refs):
-    own = refs[0]
-    parts = refs[1 : 1 + peers]
-    bias, gain, norm, maxval, matrix, ones = refs[1 + peers : 7 + peers]
-    earlier = refs[7 + peers : 7 + peers + 2 * before]
+    firsts, seconds = refs[:peers], refs[peers : 2 * peers]
+    bias, gain, norm, maxval, matrix, ones = refs[2 * peers : 2 * peers + 6]
+    earlier = refs[2 * peers + 6 : 2 * peers + 6 + 2 * before]
     (hidden, norm_out, max_out, kw_out, v_out, dec_out, mp_s, part_s, wide_s, tall_s) = refs[-10:]
     heads = matrix.shape[1]
-    rows, real = own.shape[0], matrix.shape[0]
+    rows, real = hidden.shape[0], matrix.shape[0]
     pairs = rows // PAD
     moves = spread(pairs, real // pairs)
     cols = heads * LANES
@@ -201,18 +271,18 @@
     norm_out, max_out = norm_out.at[before], max_out.at[before]
 
     scales, packed, squares = [], 0.0, 0.0
-    for part in (own,) + tuple(parts):
-        tile = part[:, 4 * cols :]
+    for part in firsts:
+        tile = part[:, 2 * cols :]
         tile = tile + lane_roll(tile, LANES // 2)
         power = tile[:, heads_all - 2 : heads_all - 1]
         scales.append(jnp.exp2(power - UP))
         packed = packed + tile * scales[-1]
         squares = squares + tile[:, heads_all - 1 : heads_all] * jnp.exp2(2.0 * power)
 
-    def total(start, width):
+    def total(parts, start):
         value = 0.0
-        for part, scale in zip((own,) + tuple(parts), scales):
-            value = value + part[:, start : start + width] * scale
+        for part, scale in zip(parts, scales):
+            value = value + part[:, start : start + LANES] * scale
         return value
 
     inv = lax.rsqrt(squares / features + norm_eps)
@@ -236,7 +306,7 @@
     part_s[...] = jnp.zeros(part_s.shape, F32)
     for h in range(heads):
         at = h * LANES
-        q = total(at, LANES) * inv
+        q = total(firsts, at) * inv
         high, rest = pieces(q)
         middle, low = pieces(rest)
         q_t = columns(high, middle, low)
@@ -249,11 +319,11 @@
                 part_s[h, (row + i) * 8 : (row + i) * 8 + 8, :] = jnp.sum(
                     product.reshape(LANES // 8, 8, LANES), axis=0
                 )
-        v = total(2 * cols + at, LANES) * inv
+        v = total(seconds, at) * inv
         v_out[h] = v
         dec = jnp.broadcast_to(decays[:, h : h + 1], (rows, LANES))
         dec_out[h] = dec
-        kw = total(cols + at, LANES) * (inv * LANES ** (-0.5)) * weight_in[:, h : h + 1]
+        kw = total(firsts, cols + at) * (inv * LANES ** (-0.5)) * weight_in[:, h : h + 1]
         kw_out[h] = kw
         for padded, plain in moves:
             nn = dec[padded] * norm[block, plain, h, :] + kw[padded]
@@ -269,20 +339,20 @@
         centred = readout - average
         variance = jnp.mean(centred * centred, axis=1, keepdims=True)
         normed = centred * lax.rsqrt(variance + head_eps) * gain[block, h : h + 1, :]
-        gate = jax.nn.sigmoid(total(3 * cols + at, LANES) * inv)
+        gate = jax.nn.sigmoid(total(seconds, cols + at) * inv)
         hidden[:, at : at + LANES] = (normed * gate).astype(BF16)
 
 
-def cell(block, own, parts, bias, gain, norm, maxval, matrix, ones, heads_all, features, earlier, last, after):
-    rows = own.shape[0]
+def cell(block, firsts, seconds, bias, gain, norm, maxval, matrix, ones, heads_all, features, earlier, last, after):
+    rows = firsts[0].shape[0]
     real, heads = matrix.shape[:2]
     whole = pl.BlockSpec(memory_space=pltpu.VMEM)
     gates = jax.ShapeDtypeStruct((heads, rows, LANES), F32)
     blocks = block + 1 if last else 1
     earlier = list(earlier) if last else []
     return pl.pallas_call(
-        functools.partial(cell_kernel, block, features, heads_all, len(parts), len(earlier) // 2),
-        in_specs=[whole] * (7 + len(parts) + len(earlier)) + [pl.BlockSpec(memory_space=pl.ANY)] * len(after),
+        functools.partial(cell_kernel, block, features, heads_all, len(firsts), len(earlier) // 2),
+        in_specs=[whole] * (6 + 2 * len(firsts) + len(earlier)) + [pl.BlockSpec(memory_space=pl.ANY)] * len(after),
         out_specs=[whole] * 6,
         out_shape=[
             jax.ShapeDtypeStruct((rows, heads * LANES), BF16),
@@ -303,7 +373,7 @@
             flops=4 * real * heads * LANES * LANES, bytes_accessed=1 << 20, transcendentals=0
         ),
         name="cell",
-    )(own, *parts, bias, gain, norm, maxval, in_vmem(matrix), in_vmem(ones), *earlier, *after)
+    )(*firsts, *seconds, bias, gain, norm, maxval, in_vmem(matrix), in_vmem(ones), *earlier, *after)
 
 
 def update_kernel(block, kw, v, dec, matrix, ones, *rest):
@@ -427,25 +497,24 @@
     current = lax.all_to_all(copied, "tp", 0, 0)
     earlier, matrix_out, after = [], None, ()
     for block in range(blocks):
-        own, *sends = project(block, meta, current, weights if block else first, dp)
-        parts = [
-            swap(part.astype(jnp.float16), "dp", dp, slot).astype(F32) for slot, part in enumerate(sends, 1)
-        ]
+        firsts, seconds = project(block, meta, current, weights if block else first, dp)
+        state = [(mem_matrix.shape[1:], F32)]
         if block == 0:
-            state = mem_matrix.shape[1:]
-            *matrices, ones = fetch(
-                (mem_matrix,), [(0, i, i, None) for i in range(blocks)], [(state, F32)] * blocks, True, (own,)
-            )
+            *matrices, ones = fetch((mem_matrix,), [(0, 0, 0, None)], state, True, (seconds[0],))
             after = tuple(matrices)
         hidden, norm_out, max_out, kw, v, dec = cell(
-            block, own, parts, forget_bias, head_gain, mem_norm, mem_max, matrices[block], ones,
+            block, firsts, seconds, forget_bias, head_gain, mem_norm, mem_max, matrices[block], ones,
             heads_all, features * dp, earlier, block + 1 == blocks, after,
         )
         earlier += [norm_out, max_out]
         gathered = [hidden] + [swap(hidden, "dp", dp, slot) for slot in range(1, dp)]
         matrix_out = update(block, blocks, kw, v, dec, matrices[block], ones, matrix_out)
         after = (in_hbm(matrix_out),)
-        partial = output(block, meta, w_proj, gathered, after if block + 1 == blocks else ()).reshape(tp, PAD, features)
+        fillers = after
+        if block + 1 < blocks:
+            fillers = fetch((mem_matrix,), [(0, block + 1, 0, None)], state, False, (hidden,))
+            matrices += fillers
+        partial = output(block, meta, w_proj, gathered, tuple(fillers)).reshape(tp, PAD, features)
         summed = lax.all_to_all(partial.astype(jnp.float16), "tp", 0, 0)
         summed = (jnp.sum(summed.astype(F32), axis=0) * (1.0 / OUT_UP)).astype(BF16)
         if block + 1 < blocks:

time: 93.9 us -> 92.3 us (0.983)
  waiting for transfers between devices: 6.7 us -> 1.76 us
  starting transfers between devices: 7.75 us -> 9.33 us
  Pallas kernels: 24.3 us -> 25.7 us
    ppermute x12 -> x14, waiting for transfers between devices: 6.7 us -> 1.76 us  [swap(): return lax.ppermute(x, axis, [(i, i ^ bit) for i in range(size)])]
    ppermute x12 -> x14, starting transfers between devices: 7.75 us -> 9.33 us  [swap(): return lax.ppermute(x, axis, [(i, i ^ bit) for i in range(size)])]
    pallas_call x1 -> x2, Pallas kernels: 5.23 us -> 6.22 us  [fetch(): pl.pallas_call(functools.partial(fetch_kernel, (steps, len(shapes), with_...]
    pallas_call x2 -> x8, Pallas kernels: 3.27 us -> 3.97 us  [small_call(): pl.pallas_call(kernel, in_specs=[pl.BlockSpec(memory_space=pltpu.SMEM)] *...]
  transfers between devices with their start and end apart: 12 -> 14, of which waited for: 5 -> 3; matrix products, arithmetic and copies ran while one was open for 0% -> 0% of each run, Pallas kernels for 14% -> 16%
where the time goes in v3:
time: 92.3 us; the launch traced here: 92 us
  blocking collectives  53.1 us (58%)
  Pallas kernels  25.7 us (28%)
  starting transfers between devices  9.33 us (10%)
  waiting for transfers between devices  1.76 us (2%)
  between operations  1.03 us (1%)
  other arithmetic  0.94 us (1%)
    all_to_all x2, blocking collectives, on_device(): summed = lax.all_to_all(partial.astype(jnp.float16), 'tp', 0, 0)  25.2 us
    all_to_all x1, blocking collectives, on_device(): current = lax.all_to_all(copied, 'tp', 0, 0)  16 us
    all_to_all x1, blocking collectives, on_device(): lax.all_to_all(jnp.broadcast_to(summed[None], (tp,) + summed.shape), 'tp'...  12 us
    ppermute x14, starting transfers between devices, swap(): return lax.ppermute(x, axis, [(i, i ^ bit) for i in range(size)])  9.33 us
    pallas_call x2, Pallas kernels, update(): pl.pallas_call(functools.partial(update_kernel, block), in_specs=[whole]...  7.38 us
    pallas_call x2, Pallas kernels, fetch(): pl.pallas_call(functools.partial(fetch_kernel, (steps, len(shapes), with_...  6.22 us
    pallas_call x8, Pallas kernels, small_call(): pl.pallas_call(kernel, in_specs=[pl.BlockSpec(memory_space=pltpu.SMEM)] *...  3.97 us
    pallas_call x2, Pallas kernels, cell(): pl.pallas_call(functools.partial(cell_kernel, block, features, heads_all,...  3.96 us
  transfers between devices with their start and end apart: 14, of which 3 were waited for; matrix products, arithmetic and copies ran while one was open for 0% of the time, Pallas kernels for 16%

profile of v3, /device:TPU:0, one launch (start us, length us, event | category | flops | bytes accessed | tf_op | source)
XLA Modules:
  0.0 92.0 jit_solution(16716773334893843044)
XLA Ops:
  0.7 2.4 %begin.1 = (bf16[8,14,1024]{2,1,0:T(8,128)(2,1)S(1)}, bf16[1,1024,512]{2,1,0:T(8,128)(2,1)S(1)}, bf16[1,1024,512]{2,1,0:T(8,128)(2,1)S(1)}, bf16[1,1024,512]{2,1...) custom-call(bf16[14,1024]{1,0:T(8,128)(2,1)} %tokens, ...), custom_call_target="tpu_custom_call" | custom-call | tf_op jit(solution)/shard_map/begin/pallas_call | solution.py:88
  3.2 16.0 %all_to_all.20.x = bf16[8,14,1024]{2,1,0:T(8,128)(2,1)S(1)} all-to-all(bf16[8,14,1024]{2,1,0:T(8,128)(2,1)S(1)} %get-tuple-element.49), channel_id=1, replica_groups=mesh['tp'=8,'dp'=4] {'tp'}, dimensions={0} | all-to-all | bytes 458752 | tf_op jit(solution)/shard_map/all_to_all | solution.py:497
  19.2 1.3 %project_first.2 = (f32[64,1152]{1,0:T(8,128)S(1)}, f32[64,1152]{1,0:T(8,128)S(1)}, bf16[128,1024]{1,0:T(8,128)(2,1)S(1)}) custom-call(s32[2]{0:T(128)S(1)} %pad_add_fusion.meta, bf16[8,14,1024]{2,1,0:T(8,128)(2,1)S(1)} %all_to_all.20.x, bf16[1,1024,512]{2,1,0:T(8,128)(2,1)S(1)} %get-tuple-element.50.wq, bf16[1,1024,512]{2,1,0:T(8,128)(2,1)S(1)} %get-tuple-element.51.wk, ...), custom_call_target="tpu_custom_call" | custom-call | flops 268435456 | bytes 1048576 | tf_op jit(solution)/shard_map/project_first/pallas_call | solution.py:174
  21.5 0.6 collective-permute-done.other
  22.3 1.6 %collective-permute-start.1 = (f16[32,1152]{1,0:T(8,128)(2,1)S(1)}, f16[32,1152]{1,0:T(8,128)(2,1)S(1)}, u32[]{:S(2)}, u32[]{:S(2)}) collective-permute-start(f16[32,1152]{1,0:T(8,128)(2,1)S(1)} %convert_element_type.52), channel_id=1, source_target_pairs={{0,2},{1,3},{2,0},{3,1},{4,6},{5,7},{6,4},{7,5},{8,10},{9,11},{10,... | collective-permute-start | bytes 221192 | tf_op jit(solution)/shard_map/ppermute | solution.py:464
  24.0 0.6 collective-permute-start.3
  24.6 3.1 %fetch.2 = (f32[28,4,128,128]{3,2,1,0:T(8,128)S(1)}, bf16[128,4096]{1,0:T(8,128)(2,1)S(1)}) custom-call(f32[2,28,4,128,128]{4,3,2,1,0:T(8,128)} %refs_0_.5, f32[32,1024]{1,0:T(8,128)S(1)} %get-tuple-element.64.refs_1_.refs_2_), custom_call_target="tpu_custom_call" | custom-call | flops 14680064 | bytes 14680064 | tf_op jit(solution)/shard_map/fetch/pallas_call | solution.py:58
  27.7 0.6 collective-permute-done.3
  28.4 1.7 %cell.2 = (bf16[32,512]{1,0:T(8,128)(2,1)S(1)}, f32[1,28,4,128]{3,2,1,0:T(4,128)S(1)}, f32[1,4,28]{2,1,0:T(4,128)S(1)}, f32[4,32,128]{2,1,0:T(8,128)S(1)}, f32[4...) custom-call(f32[32,1152]{1,0:T(8,128)S(1)} %get-tuple-element.56.refs_0_, f32[32,1152]{1,0:T(8,128)S(1)} %convert_element_type.53.refs_1_, ...), custom_call_target="tpu_custom_call" | custom-call | flops 7340032 | bytes 1048576 | tf_op jit(solution)/shard_map/cell/pallas_call | solution.py:353
  30.3 1.2 %collective-permute-start.5 = (bf16[32,512]{1,0:T(8,128)(2,1)S(1)}, bf16[32,512]{1,0:T(8,128)(2,1)S(1)}, u32[]{:S(2)}, u32[]{:S(2)}) collective-permute-start(bf16[32,512]{1,0:T(8,128)(2,1)S(1)} %get-tuple-element.68.refs_1_.refs_0_), channel_id=1, source_target_pairs={{0,2},{1,3},{2,0},{3,1},{4,6},{5,7},{6,4},{7,5},{8,10},{9,11},{10,... | collective-permute-start | bytes 98312 | tf_op jit(solution)/shard_map/ppermute | solution.py:464
  32.0 3.1 %fetch.3.refs_4_.refs_8_.matrix = f32[28,4,128,128]{3,2,1,0:T(8,128)S(1)} custom-call(f32[2,28,4,128,128]{4,3,2,1,0:T(8,128)} %refs_0_.5, bf16[32,512]{1,0:T(8,128)(2,1)S(1)} %get-tuple-element.68.refs_1_.refs_0_), custom_call_target="tpu_custom_call" | custom-call | flops 14680064 | bytes 14680064 | tf_op jit(solution)/shard_map/fetch/pallas_call | solution.py:58
  35.2 0.9 output.2
  36.1 12.7 %all_to_all.21 = f16[8,16,1024]{2,1,0:T(8,128)(2,1)S(1)} all-to-all(f16[8,16,1024]{2,1,0:T(8,128)(2,1)S(1)} %bitcast.14), channel_id=1, replica_groups=mesh['tp'=8,'dp'=4] {'tp'}, dimensions={0} | all-to-all | bytes 524288 | tf_op jit(solution)/shard_map/all_to_all | solution.py:518
  48.9 12.0 %all_to_all.22.x = bf16[8,16,1024]{2,1,0:T(8,128)(2,1)S(1)} all-to-all(bf16[8,16,1024]{2,1,0:T(8,128)(2,1)S(1)} %broadcast_in_dim.2), channel_id=1, replica_groups=mesh['tp'=8,'dp'=4] {'tp'}, dimensions={0} | all-to-all | bytes 524288 | tf_op jit(solution)/shard_map/all_to_all | solution.py:521
  60.9 1.3 %project_first.3 = (f32[64,1152]{1,0:T(8,128)S(1)}, f32[64,1152]{1,0:T(8,128)S(1)}, bf16[128,1024]{1,0:T(8,128)(2,1)S(1)}) custom-call(s32[2]{0:T(128)S(1)} %pad_add_fusion.meta, bf16[8,16,1024]{2,1,0:T(8,128)(2,1)S(1)} %all_to_all.22.x, bf16[2,1024,512]{2,1,0:T(8,128)(2,1)S(1)} %copy-done.1, bf16[2,1024,512]{2,1,0:T(8,128)(2,1)S(1)} %copy-done.2, ...), custom_call_target="tpu_custom_call" | custom-call | flops 268435456 | bytes 1048576 | tf_op jit(solution)/shard_map/project_first/pallas_call | solution.py:174
  64.0 1.3 %collective-permute-start.8 = (f16[32,1152]{1,0:T(8,128)(2,1)S(1)}, f16[32,1152]{1,0:T(8,128)(2,1)S(1)}, u32[]{:S(2)}, u32[]{:S(2)}) collective-permute-start(f16[32,1152]{1,0:T(8,128)(2,1)S(1)} %convert_element_type.60), channel_id=1, source_target_pairs={{0,2},{1,3},{2,0},{3,1},{4,6},{5,7},{6,4},{7,5},{8,10},{9,11},{10,... | collective-permute-start | bytes 221192 | tf_op jit(solution)/shard_map/ppermute | solution.py:464
  65.5 0.8 collective-permute-start.10
  66.3 3.7 %update.2.refs_12_.rest_0_ = f32[2,28,4,128,128]{4,3,2,1,0:T(8,128)} custom-call(f32[4,32,128]{2,1,0:T(8,128)S(1)} %get-tuple-element.81.kw, f32[4,32,128]{2,1,0:T(8,128)S(1)} %get-tuple-element.82.v, f32[4,32,128]{2,1,0:T(8,128)S(1)} %get-tuple-element.83.dec, f32[28,4,128,128]{3,2,1,0:T(8,128)S(1)} %get-tuple-element.66.refs_8_.refs_10_.matrix, ...), custom_call_target="tpu_custom_call" | custom-call | flops 14680064 | bytes 7340032 | tf_op jit(solution)/shard_map/update/pallas_call | solution.py:408
  70.1 2.3 %cell.3 = (bf16[32,512]{1,0:T(8,128)(2,1)S(1)}, f32[2,28,4,128]{3,2,1,0:T(4,128)}, f32[2,4,28]{2,1,0:T(4,128)}, f32[4,32,128]{2,1,0:T(8,128)S(1)}, f32[4,32,128]{2,1,0:T(8,128)S(1)}, /*index=5*/f32[4,32,128]{2,1,0:T(8,128)S(1)}) custom-call(f32[32,1152]{1,0:T(8,128)S(1)} %get-tuple-element.71.refs_0_, f32[32,1152]{1,0:T(8,128)S(1)} %convert_element_type.61.refs_1_, ...), custom_call_target="tpu_custom_call" | custom-call | flops 7340032 | bytes 1048576 | tf_op jit(solution)/shard_map/cell/pallas_call | solution.py:353
  72.8 0.8 collective-permute-start.12
  74.2 3.7 %update.3.refs_4_ = f32[2,28,4,128,128]{4,3,2,1,0:T(8,128)} custom-call(f32[4,32,128]{2,1,0:T(8,128)S(1)} %get-tuple-element.85.kw, f32[4,32,128]{2,1,0:T(8,128)S(1)} %get-tuple-element.86.v, f32[4,32,128]{2,1,0:T(8,128)S(1)} %get-tuple-element.87.dec, f32[28,4,128,128]{3,2,1,0:T(8,128)S(1)} %fetch.3.refs_4_.refs_8_.matrix, ...), custom_call_target="tpu_custom_call", output_to_operand_aliasing={{}: (5, {})} | custom-call | flops 14680064 | bytes 7340032 | tf_op jit(solution)/shard_map/update/pallas_call | solution.py:408
  77.9 0.9 output.3
  78.9 12.5 %all_to_all.23 = f16[8,16,1024]{2,1,0:T(8,128)(2,1)S(1)} all-to-all(f16[8,16,1024]{2,1,0:T(8,128)(2,1)S(1)} %bitcast.15), channel_id=1, replica_groups=mesh['tp'=8,'dp'=4] {'tp'}, dimensions={0} | all-to-all | bytes 524288 | tf_op jit(solution)/shard_map/all_to_all | solution.py:518
  91.4 0.6 fusion
  (63 shorter events, 5.4 us)
Async XLA Ops:
  20.4 1.6 %collective-permute-start = (f32[64,1152]{1,0:T(8,128)S(1)}, f32[64,1152]{1,0:T(8,128)S(1)}, u32[]{:S(2)}, u32[]{:S(2)}) collective-permute-start(f32[64,1152]{1,0:T(8,128)S(1)} %get-tuple-element.55), channel_id=1, source_target_pairs={{0,1},{1,0},{2,3},{3,2},{4,5},{5,4},{6,7},{7,6},{8,9},{9,8},{10,11... | collective-permute-start | bytes 884744 | tf_op jit(solution)/shard_map/ppermute | solution.py:464
  21.0 2.9 %collective-permute-start.2 = (f32[64,1024]{1,0:T(8,128)S(1)}, f32[64,1024]{1,0:T(8,128)S(1)}, u32[]{:S(2)}, u32[]{:S(2)}) collective-permute-start(f32[64,1024]{1,0:T(8,128)S(1)} %get-tuple-element.62), channel_id=1, source_target_pairs={{0,1},{1,0},{2,3},{3,2},{4,5},{5,4},{6,7},{7,6},{8,9},{9,8},{10,11... | collective-permute-start | bytes 786440 | tf_op jit(solution)/shard_map/ppermute | solution.py:464
  22.3 6.0 %collective-permute-start.1 = (f16[32,1152]{1,0:T(8,128)(2,1)S(1)}, f16[32,1152]{1,0:T(8,128)(2,1)S(1)}, u32[]{:S(2)}, u32[]{:S(2)}) collective-permute-start(f16[32,1152]{1,0:T(8,128)(2,1)S(1)} %convert_element_type.52), channel_id=1, source_target_pairs={{0,2},{1,3},{2,0},{3,1},{4,6},{5,7},{6,4},{7,5},{8,10},{9,11},{10,... | collective-permute-start | bytes 221192 | tf_op jit(solution)/shard_map/ppermute | solution.py:464
  24.0 4.3 %collective-permute-start.3 = (f16[32,1024]{1,0:T(8,128)(2,1)S(1)}, f16[32,1024]{1,0:T(8,128)(2,1)S(1)}, u32[]{:S(2)}, u32[]{:S(2)}) collective-permute-start(f16[32,1024]{1,0:T(8,128)(2,1)S(1)} %convert_element_type.54), channel_id=1, source_target_pairs={{0,2},{1,3},{2,0},{3,1},{4,6},{5,7},{6,4},{7,5},{8,10},{9,11},{10,... | collective-permute-start | bytes 196616 | tf_op jit(solution)/shard_map/ppermute | solution.py:464
  24.5 3.8 %copy-start.8 = (f32[2,4,128]{2,1,0:T(4,128)S(1)}, f32[2,4,128]{2,1,0:T(4,128)}, u32[]{:S(2)}) copy-start(f32[2,4,128]{2,1,0:T(4,128)} %refs_5_.3) | copy-start | bytes 12292
  24.6 3.8 %copy-start.9 = (f32[2,28,4]{1,2,0:T(4,128)S(1)}, f32[2,28,4]{1,2,0:T(4,128)}, u32[]{:S(2)}) copy-start(f32[2,28,4]{1,2,0:T(4,128)} %param.25) | copy-start | bytes 2692
  24.6 3.8 %copy-start.10 = (f32[2,4]{1,0:T(2,128)S(1)}, f32[2,4]{1,0:T(2,128)}, u32[]{:S(2)}) copy-start(f32[2,4]{1,0:T(2,128)} %refs_4_.3) | copy-start | bytes 100
  30.1 5.1 %copy-start = (bf16[2,512,1024]{2,1,0:T(8,128)(2,1)S(1)}, bf16[2,512,1024]{2,1,0:T(8,128)(2,1)}, u32[]{:S(2)}) copy-start(bf16[2,512,1024]{2,1,0:T(8,128)(2,1)} %w.3) | copy-start | bytes 6291460
  30.1 5.1 %collective-permute-start.6 = (bf16[32,512]{1,0:T(8,128)(2,1)S(1)}, bf16[32,512]{1,0:T(8,128)(2,1)S(1)}, u32[]{:S(2)}, u32[]{:S(2)}) collective-permute-start(bf16[32,512]{1,0:T(8,128)(2,1)S(1)} %get-tuple-element.68.refs_1_.refs_0_), channel_id=1, source_target_pairs={{0,3},{1,2},{2,1},{3,0},{4,7},{5,6},{6,5},{7,4},{8,11},{9,10},{10,... | collective-permute-start | bytes 98312 | tf_op jit(solution)/shard_map/ppermute | solution.py:464
  30.3 4.9 %collective-permute-start.5 = (bf16[32,512]{1,0:T(8,128)(2,1)S(1)}, bf16[32,512]{1,0:T(8,128)(2,1)S(1)}, u32[]{:S(2)}, u32[]{:S(2)}) collective-permute-start(bf16[32,512]{1,0:T(8,128)(2,1)S(1)} %get-tuple-element.68.refs_1_.refs_0_), channel_id=1, source_target_pairs={{0,2},{1,3},{2,0},{3,1},{4,6},{5,7},{6,4},{7,5},{8,10},{9,11},{10,... | collective-permute-start | bytes 98312 | tf_op jit(solution)/shard_map/ppermute | solution.py:464
  31.5 3.7 %collective-permute-start.4 = (bf16[32,512]{1,0:T(8,128)(2,1)S(1)}, bf16[32,512]{1,0:T(8,128)(2,1)S(1)}, u32[]{:S(2)}, u32[]{:S(2)}) collective-permute-start(bf16[32,512]{1,0:T(8,128)(2,1)S(1)} %get-tuple-element.68.refs_1_.refs_0_), channel_id=1, source_target_pairs={{0,1},{1,0},{2,3},{3,2},{4,5},{5,4},{6,7},{7,6},{8,9},{9,8},{10,11... | collective-permute-start | bytes 98312 | tf_op jit(solution)/shard_map/ppermute | solution.py:464
  35.1 25.8 %copy-start.1 = (bf16[2,1024,512]{2,1,0:T(8,128)(2,1)S(1)}, bf16[2,1024,512]{2,1,0:T(8,128)(2,1)}, u32[]{:S(2)}) copy-start(bf16[2,1024,512]{2,1,0:T(8,128)(2,1)} %wq.1) | copy-start | bytes 6291460
  35.1 25.8 %copy-start.2 = (bf16[2,1024,512]{2,1,0:T(8,128)(2,1)S(1)}, bf16[2,1024,512]{2,1,0:T(8,128)(2,1)}, u32[]{:S(2)}) copy-start(bf16[2,1024,512]{2,1,0:T(8,128)(2,1)} %wk.1) | copy-start | bytes 6291460
  35.1 25.8 %copy-start.5 = (bf16[2,1024,32]{1,2,0:T(8,128)(2,1)S(1)}, bf16[2,1024,32]{1,2,0:T(8,128)(2,1)}, u32[]{:S(2)}) copy-start(bf16[2,1024,32]{1,2,0:T(8,128)(2,1)} %param.18) | copy-start | bytes 393220
  35.1 25.8 %copy-start.6 = (bf16[2,1024,32]{1,2,0:T(8,128)(2,1)S(1)}, bf16[2,1024,32]{1,2,0:T(8,128)(2,1)}, u32[]{:S(2)}) copy-start(bf16[2,1024,32]{1,2,0:T(8,128)(2,1)} %param.19) | copy-start | bytes 393220
  35.1 27.1 %copy-start.3 = (bf16[2,1024,512]{2,1,0:T(8,128)(2,1)S(1)}, bf16[2,1024,512]{2,1,0:T(8,128)(2,1)}, u32[]{:S(2)}) copy-start(bf16[2,1024,512]{2,1,0:T(8,128)(2,1)} %wv.1) | copy-start | bytes 6291460
  35.2 27.1 %copy-start.4 = (bf16[2,1024,512]{2,1,0:T(8,128)(2,1)S(1)}, bf16[2,1024,512]{2,1,0:T(8,128)(2,1)}, u32[]{:S(2)}) copy-start(bf16[2,1024,512]{2,1,0:T(8,128)(2,1)} %wo.1) | copy-start | bytes 6291460
  62.2 1.6 %collective-permute-start.7 = (f32[64,1152]{1,0:T(8,128)S(1)}, f32[64,1152]{1,0:T(8,128)S(1)}, u32[]{:S(2)}, u32[]{:S(2)}) collective-permute-start(f32[64,1152]{1,0:T(8,128)S(1)} %get-tuple-element.70), channel_id=1, source_target_pairs={{0,1},{1,0},{2,3},{3,2},{4,5},{5,4},{6,7},{7,6},{8,9},{9,8},{10,11... | collective-permute-start | bytes 884744 | tf_op jit(solution)/shard_map/ppermute | solution.py:464
  62.7 2.6 %collective-permute-start.9 = (f32[64,1024]{1,0:T(8,128)S(1)}, f32[64,1024]{1,0:T(8,128)S(1)}, u32[]{:S(2)}, u32[]{:S(2)}) collective-permute-start(f32[64,1024]{1,0:T(8,128)S(1)} %get-tuple-element.75), channel_id=1, source_target_pairs={{0,1},{1,0},{2,3},{3,2},{4,5},{5,4},{6,7},{7,6},{8,9},{9,8},{10,11... | collective-permute-start | bytes 786440 | tf_op jit(solution)/shard_map/ppermute | solution.py:464
  64.0 6.0 %collective-permute-start.8 = (f16[32,1152]{1,0:T(8,128)(2,1)S(1)}, f16[32,1152]{1,0:T(8,128)(2,1)S(1)}, u32[]{:S(2)}, u32[]{:S(2)}) collective-permute-start(f16[32,1152]{1,0:T(8,128)(2,1)S(1)} %convert_element_type.60), channel_id=1, source_target_pairs={{0,2},{1,3},{2,0},{3,1},{4,6},{5,7},{6,4},{7,5},{8,10},{9,11},{10,... | collective-permute-start | bytes 221192 | tf_op jit(solution)/shard_map/ppermute | solution.py:464
  65.5 4.5 %collective-permute-start.10 = (f16[32,1024]{1,0:T(8,128)(2,1)S(1)}, f16[32,1024]{1,0:T(8,128)(2,1)S(1)}, u32[]{:S(2)}, u32[]{:S(2)}) collective-permute-start(f16[32,1024]{1,0:T(8,128)(2,1)S(1)} %convert_element_type.62), channel_id=1, source_target_pairs={{0,2},{1,3},{2,0},{3,1},{4,6},{5,7},{6,4},{7,5},{8,10},{9,11},{10,... | collective-permute-start | bytes 196616 | tf_op jit(solution)/shard_map/ppermute | solution.py:464
  72.3 5.6 %collective-permute-start.13 = (bf16[32,512]{1,0:T(8,128)(2,1)S(1)}, bf16[32,512]{1,0:T(8,128)(2,1)S(1)}, u32[]{:S(2)}, u32[]{:S(2)}) collective-permute-start(bf16[32,512]{1,0:T(8,128)(2,1)S(1)} %get-tuple-element.84.refs_0_), channel_id=1, source_target_pairs={{0,3},{1,2},{2,1},{3,0},{4,7},{5,6},{6,5},{7,4},{8,11},{9,10},{10,... | collective-permute-start | bytes 98312 | tf_op jit(solution)/shard_map/ppermute | solution.py:464
  72.8 5.1 %collective-permute-start.12 = (bf16[32,512]{1,0:T(8,128)(2,1)S(1)}, bf16[32,512]{1,0:T(8,128)(2,1)S(1)}, u32[]{:S(2)}, u32[]{:S(2)}) collective-permute-start(bf16[32,512]{1,0:T(8,128)(2,1)S(1)} %get-tuple-element.84.refs_0_), channel_id=1, source_target_pairs={{0,2},{1,3},{2,0},{3,1},{4,6},{5,7},{6,4},{7,5},{8,10},{9,11},{10,... | collective-permute-start | bytes 98312 | tf_op jit(solution)/shard_map/ppermute | solution.py:464
  73.7 4.3 %collective-permute-start.11 = (bf16[32,512]{1,0:T(8,128)(2,1)S(1)}, bf16[32,512]{1,0:T(8,128)(2,1)S(1)}, u32[]{:S(2)}, u32[]{:S(2)}) collective-permute-start(bf16[32,512]{1,0:T(8,128)(2,1)S(1)} %get-tuple-element.84.refs_0_), channel_id=1, source_target_pairs={{0,1},{1,0},{2,3},{3,2},{4,5},{5,4},{6,7},{7,6},{8,9},{9,8},{10,11... | collective-permute-start | bytes 98312 | tf_op jit(solution)/shard_map/ppermute | solution.py:464
  (1 other events, 3.8 us)

commit v4 on v3

--- a/solution.py
+++ b/solution.py
@@ -14,6 +14,7 @@
 LANES = 128
 UP = 12.0
 TINY = 1e-30
+STORES = 2
 OUT_UP = 16.0
 F32 = jnp.float32
 BF16 = jnp.bfloat16
@@ -96,11 +97,17 @@
     )(*map(in_hbm, (tokens,) + weights))
 
 
-def first_project_kernel(block, heads_all, meta, x, wq, wk, wi, wf, keep, send, x_rel, gates):
+def first_project_kernel(block, heads_all, heads, x, wq, wk, wi, wf, *rest):
+    later = (len(rest) - 5) // 2
+    keep, send, x_rel, gates = rest[later : later + 3] + (rest[2 * later + 3],)
+    copies = []
+    for source, target in zip(rest[:later], rest[later + 3 : 2 * later + 3]):
+        copies.append(pltpu.make_async_copy(source.at[:1], target, rest[-1].at[len(copies)]))
+        copies[-1].start()
     rows = ROWS
     slots = x_rel.shape[0] // rows
-    me = meta[0]
-    first_head = meta[1]
+    me = lax.axis_index("dp")
+    first_head = lax.axis_index("tp") * heads
     pairs, real = rows // PAD, x.shape[1]
     if real < PAD:
         x_rel[...] = jnp.zeros(x_rel.shape, BF16)
@@ -128,6 +135,8 @@
     lane = lax.broadcasted_iota(jnp.int32, gates.shape, 1)
     mine = pltpu.roll(gates[...], (LANES - first_head) % LANES, 1)
     emit(jnp.where(lane == heads_all - 1, squares, mine), 2 * cols)
+    for copy in copies:
+        copy.wait()
 
 
 def second_project_kernel(block, x_rel, wv, wo, keep, send):
@@ -169,13 +178,13 @@
     return list(range(0, slots, 2)) + list(range(1, slots, 2))
 
 
-def small_call(kernel, name, shapes, args, scratch=(), scalars=0, flops=0):
+def small_call(kernel, name, shapes, args, scratch=(), in_place=0, flops=0):
     whole = pl.BlockSpec(memory_space=pltpu.VMEM)
     return pl.pallas_call(
         kernel,
-        in_specs=[pl.BlockSpec(memory_space=pltpu.SMEM)] * scalars + [whole] * (len(args) - scalars),
+        in_specs=[whole] * (len(args) - in_place) + [pl.BlockSpec(memory_space=pltpu.HBM)] * in_place,
         out_specs=[whole] * len(shapes),
-        out_shape=[jax.ShapeDtypeStruct(shape, dtype) for shape, dtype in shapes],
+        out_shape=[pltpu.VMEM(shape, dtype) for shape, dtype in shapes],
         scratch_shapes=list(scratch),
         compiler_params=pltpu.CompilerParams(vmem_limit_bytes=8 << 20),
         cost_estimate=pl.CostEstimate(flops=flops, bytes_accessed=1 << 20, transcendentals=0),
@@ -183,22 +192,27 @@
     )(*args)
 
 
-def project(block, meta, x, weights, slots):
-    wq, wk, wv, wo, wi, wf = map(in_vmem, weights)
+def project(block, heads, x, weights, later, slots):
+    wq, wk, wi, wf, *others = map(in_vmem, weights)
+    later = [in_hbm(w) for w in later]
     all_rows, features = slots * ROWS, x.shape[2]
     half = all_rows // 2
     cols, heads_all = wq.shape[2], wi.shape[1]
     first, second = 2 * cols + LANES, 2 * cols
     flops = 2 * all_rows * features * second
-    keep_a, send_a, x_rel = small_call(
-        functools.partial(first_project_kernel, block, heads_all),
+    scratch = [pltpu.VMEM((all_rows, LANES), F32), pltpu.SemaphoreType.DMA((max(len(later), 1),))]
+    keep_a, send_a, x_rel, *fetched = small_call(
+        functools.partial(first_project_kernel, block, heads_all, heads),
         "project_first",
-        [((half, first), F32)] * 2 + [((all_rows, features), BF16)],
-        (meta, x, wq, wk, wi, wf),
-        [pltpu.VMEM((all_rows, LANES), F32)],
-        1,
+        [((half, first), F32)] * 2
+        + [((all_rows, features), BF16)]
+        + [((1,) + w.shape[1:], BF16) for w in later],
+        (x, wq, wk, wi, wf, *later),
+        scratch,
+        len(later),
         flops,
     )
+    wv, wo = fetched or others
     other_a = swap(send_a, "dp", slots, 1)
     keep_b, send_b = small_call(
         functools.partial(second_project_kernel, block),
@@ -347,7 +361,7 @@
     rows = firsts[0].shape[0]
     real, heads = matrix.shape[:2]
     whole = pl.BlockSpec(memory_space=pltpu.VMEM)
-    gates = jax.ShapeDtypeStruct((heads, rows, LANES), F32)
+    gates = pltpu.VMEM((heads, rows, LANES), F32)
     blocks = block + 1 if last else 1
     earlier = list(earlier) if last else []
     return pl.pallas_call(
@@ -355,9 +369,9 @@
         in_specs=[whole] * (6 + 2 * len(firsts) + len(earlier)) + [pl.BlockSpec(memory_space=pl.ANY)] * len(after),
         out_specs=[whole] * 6,
         out_shape=[
-            jax.ShapeDtypeStruct((rows, heads * LANES), BF16),
-            jax.ShapeDtypeStruct((blocks,) + norm.shape[1:], F32),
-            jax.ShapeDtypeStruct((blocks,) + maxval.shape[1:], F32),
+            pltpu.VMEM((rows, heads * LANES), BF16),
+            pltpu.VMEM((blocks,) + norm.shape[1:], F32),
+            pltpu.VMEM((blocks,) + maxval.shape[1:], F32),
             gates,
             gates,
             gates,
@@ -383,6 +397,7 @@
     moves = spread(pairs, real // pairs)
     copies = []
     for h in range(heads):
+        start = 0
         k_high, k_low = pieces(kw[h])
         k_t = columns(k_high, k_high, k_low)
         v_high, v_low = pieces(v[h])
@@ -395,8 +410,16 @@
             for i in range(count):
                 decay = dec[h, row + i : row + i + 1, :]
                 buffer[h, seq + i] = decay * matrix[seq + i, h] + outer[:, i * LANES : (i + 1) * LANES]
-        copies.append(pltpu.make_async_copy(buffer.at[h], out.at[block, :, h], sems.at[h]))
-        copies[-1].start()
+            done = seq + count
+            if done * STORES % real < count * STORES:
+                part = pl.ds(start, done - start)
+                copies.append(
+                    pltpu.make_async_copy(
+                        buffer.at[h, part], out.at[block, part, h], sems.at[len(copies)]
+                    )
+                )
+                copies[-1].start()
+                start = done
     for copy in copies:
         copy.wait()
 
@@ -413,7 +436,7 @@
         input_output_aliases={5: 0} if aliased else {},
         scratch_shapes=[
             pltpu.VMEM((heads, real, LANES, LANES), F32),
-            pltpu.SemaphoreType.DMA((heads,)),
+            pltpu.SemaphoreType.DMA((heads * (STORES + 1),)),
         ],
         compiler_params=pltpu.CompilerParams(vmem_limit_bytes=12 << 20),
         cost_estimate=pl.CostEstimate(
@@ -425,39 +448,33 @@
     )(kw, v, dec, in_vmem(matrix), in_vmem(ones), *map(in_hbm, aliased))
 
 
-def output_kernel(slots, meta, w, *refs):
+def output_kernel(block, slots, w, *refs):
     parts, out = refs[:slots], refs[-1]
     rows = parts[0].shape[0]
-    me = meta[0]
+    me = lax.axis_index("dp")
     value = jnp.dot(
-        jnp.concatenate([part[...] for part in parts], axis=0), w[0], preferred_element_type=F32
+        jnp.concatenate([part[...] for part in parts], axis=0), w[block], preferred_element_type=F32
     )
     value = value * OUT_UP
-    for slot in range(len(parts)):
+    for slot in range(slots):
         start = pl.multiple_of((me ^ slot) * rows, rows)
         out[pl.ds(start, rows), :] = value[slot * rows : (slot + 1) * rows]
 
 
-def output(block, meta, w, parts, after):
+def output(block, w, parts, after):
     rows = parts[0].shape[0]
     whole = pl.BlockSpec(memory_space=pltpu.VMEM)
     return pl.pallas_call(
-        functools.partial(output_kernel, len(parts)),
-        in_specs=[
-            pl.BlockSpec(memory_space=pltpu.SMEM),
-            pl.BlockSpec((1,) + w.shape[1:], lambda i: (block, 0, 0)),
-        ]
-        + [whole] * len(parts)
-        + [pl.BlockSpec(memory_space=pl.ANY)] * len(after),
-        grid=(1,),
+        functools.partial(output_kernel, block, len(parts)),
+        in_specs=[whole] * (1 + len(parts)) + [pl.BlockSpec(memory_space=pl.ANY)] * len(after),
         out_specs=whole,
-        out_shape=jax.ShapeDtypeStruct((rows * len(parts), w.shape[2]), F32),
-        compiler_params=pltpu.CompilerParams(vmem_limit_bytes=12 << 20),
+        out_shape=pltpu.VMEM((rows * len(parts), w.shape[2]), F32),
+        compiler_params=pltpu.CompilerParams(vmem_limit_bytes=8 << 20),
         cost_estimate=pl.CostEstimate(
             flops=2 * rows * len(parts) * w.shape[1] * w.shape[2], bytes_accessed=1 << 20, transcendentals=0
         ),
         name="output",
-    )(meta, w, *parts, *after)
+    )(in_vmem(w), *parts, *after)
 
 
 def swap(x, axis, size, bit):
@@ -486,18 +503,18 @@
     heads_all = w_ingate.shape[2]
     assert dp & (dp - 1) == 0 and tp % dp == 0 and real <= PAD and 2 * heads_all <= LANES // 2
     assert tp // dp * PAD == ROWS and heads < heads_all - 2
-    meta = jnp.stack([lax.axis_index("dp"), lax.axis_index("tp") * heads]).astype(jnp.int32)
-
     w_ingate, w_forget = w_ingate.swapaxes(1, 2), w_forget.swapaxes(1, 2)
     mem_max = mem_max.swapaxes(1, 2)
     blocks = w_query.shape[0]
-    weights = (w_query, w_key, w_value, w_outgate, w_ingate, w_forget)
-    tokens, meta = lax.optimization_barrier((tokens, meta))
+    weights, later = (w_query, w_key, w_ingate, w_forget), (w_value, w_outgate)
     copied, *first = begin(tokens, weights, tp)
     current = lax.all_to_all(copied, "tp", 0, 0)
     earlier, matrix_out, after = [], None, ()
     for block in range(blocks):
-        firsts, seconds = project(block, meta, current, weights if block else first, dp)
+        if block == 0:
+            firsts, seconds = project(block, heads, current, first, later, dp)
+        else:
+            firsts, seconds = project(block, heads, current, weights + later, (), dp)
         state = [(mem_matrix.shape[1:], F32)]
         if block == 0:
             *matrices, ones = fetch((mem_matrix,), [(0, 0, 0, None)], state, True, (seconds[0],))
@@ -514,7 +531,7 @@
         if block + 1 < blocks:
             fillers = fetch((mem_matrix,), [(0, block + 1, 0, None)], state, False, (hidden,))
             matrices += fillers
-        partial = output(block, meta, w_proj, gathered, tuple(fillers)).reshape(tp, PAD, features)
+        partial = output(block, w_proj, gathered, tuple(fillers)).reshape(tp, PAD, features)
         summed = lax.all_to_all(partial.astype(jnp.float16), "tp", 0, 0)
         summed = (jnp.sum(summed.astype(F32), axis=0) * (1.0 / OUT_UP)).astype(BF16)
         if block + 1 < blocks:

time: 92.3 us -> 90.6 us (0.982)
  blocking collectives: 53.1 us -> 40.7 us
  waiting for transfers between devices: 1.76 us -> 9.67 us
  starting transfers between devices: 9.33 us -> 13 us
  Pallas kernels: 25.7 us -> 23 us
  local copies, waits for them, and re-layouts: 0.08 us -> 1.31 us
    all_to_all x2 -> x1, blocking collectives: 25.2 us -> 12.7 us  [on_device(): summed = lax.all_to_all(partial.astype(jnp.float16), 'tp', 0, 0)]
    all_to_all x0 -> x1, waiting for transfers between devices: none -> 7.89 us  [on_device(): summed = lax.all_to_all(partial.astype(jnp.float16), 'tp', 0, 0)]
    all_to_all x0 -> x1, starting transfers between devices: none -> 3.59 us  [on_device(): summed = lax.all_to_all(partial.astype(jnp.float16), 'tp', 0, 0)]
    pallas_call x10, Pallas kernels: 5.69 us -> 4.38 us  [the longest x8 3.75 us: small_call(): pl.pallas_call(kernel, in_specs=[whole] * (len(args) - in_place) + [pl.Bl...]
    unnamed x22 -> x24, local copies, waits for them, and re-layouts: 0.06 us -> 1.29 us
  transfers between devices with their start and end apart: 14 -> 15, of which waited for: 3 -> 4; matrix products, arithmetic and copies ran while one was open for 0% -> 1% of each run, Pallas kernels for 16% -> 16%
where the time goes in v4:
time: 90.6 us; the launch traced here: 90.2 us
  blocking collectives  40.7 us (45%)
  Pallas kernels  23 us (25%)
  starting transfers between devices  13 us (14%)
  waiting for transfers between devices  9.67 us (11%)
  other arithmetic  1.55 us (2%)
  local copies, waits for them, and re-layouts  1.31 us (1%)
  between operations  1.02 us (1%)
    all_to_all x1, blocking collectives, on_device(): current = lax.all_to_all(copied, 'tp', 0, 0)  16 us
    all_to_all x1, blocking collectives, on_device(): summed = lax.all_to_all(partial.astype(jnp.float16), 'tp', 0, 0)  12.7 us
    all_to_all x1, blocking collectives, on_device(): lax.all_to_all(jnp.broadcast_to(summed[None], (tp,) + summed.shape), 'tp'...  12 us
    ppermute x14, starting transfers between devices, swap(): return lax.ppermute(x, axis, [(i, i ^ bit) for i in range(size)])  9.4 us
    all_to_all x1, waiting for transfers between devices, on_device(): summed = lax.all_to_all(partial.astype(jnp.float16), 'tp', 0, 0)  7.89 us
    pallas_call x2, Pallas kernels, update(): pl.pallas_call(functools.partial(update_kernel, block), in_specs=[whole]...  7.07 us
    pallas_call x2, Pallas kernels, fetch(): pl.pallas_call(functools.partial(fetch_kernel, (steps, len(shapes), with_...  6.22 us
    pallas_call x8, Pallas kernels, small_call(): pl.pallas_call(kernel, in_specs=[whole] * (len(args) - in_place) + [pl.Bl...  3.75 us
  transfers between devices with their start and end apart: 15, of which 4 were waited for; matrix products, arithmetic and copies ran while one was open for 1% of the time, Pallas kernels for 16%

profile of v4, /device:TPU:0, one launch (start us, length us, event | category | flops | bytes accessed | tf_op | source)
XLA Modules:
  0.0 90.2 jit_solution(14905763726328029746)
XLA Ops:
  0.6 1.8 %begin.1 = (bf16[8,14,1024]{2,1,0:T(8,128)(2,1)S(1)}, bf16[1,1024,512]{2,1,0:T(8,128)(2,1)S(1)}, bf16[1,1024,512]{2,1,0:T(8,128)(2,1)S(1)}, bf16[1,32,1024]{2,1,0:T(8,128)(2,1)S(1)}, bf16[1,32,1024]{2,1,0:T(8,128)(2,1)S(1)}) custom-call(bf16[14,1024]{1,0:T(8,128)(2,1)} %tokens.1, bf16[2,1024,512]{2,1,0:T(8,128)(2,1)} %wq.1, bf16[2,1024,512]{2,1,0:T(8,128)(2,1)} %wk.1, ...), custom_call_target="tpu_custom_call" | custom-call | tf_op jit(solution)/shard_map/begin/pallas_call | solution.py:89
  2.4 16.0 %all_to_all.20.x = bf16[8,14,1024]{2,1,0:T(8,128)(2,1)S(1)} all-to-all(bf16[8,14,1024]{2,1,0:T(8,128)(2,1)S(1)} %get-tuple-element.45), channel_id=1, replica_groups=mesh['tp'=8,'dp'=4] {'tp'}, dimensions={0} | all-to-all | bytes 458752 | tf_op jit(solution)/shard_map/all_to_all | solution.py:511
  18.4 1.6 %project_first.2 = (f32[64,1152]{1,0:T(8,128)S(1)}, f32[64,1152]{1,0:T(8,128)S(1)}, bf16[128,1024]{1,0:T(8,128)(2,1)S(1)}, bf16[1,1024,512]{2,1,0:T(8,128)(2,1)S(1)}, bf16[1,1024,512]{2,1,0:T(8,128)(2,1)S(1)}) custom-call(bf16[8,14,1024]{2,1,0:T(8,128)(2,1)S(1)} %all_to_all.20.x, bf16[1,1024,512]{2,1,0:T(8,128)(2,1)S(1)} %get-tuple-element.46.wq, ...), custom_call_target="tpu_custom_call" | custom-call | flops 268435456 | bytes 1048576 | tf_op jit(solution)/shard_map/project_first/pallas_call | solution.py:183
  21.9 1.6 %collective-permute-start.1 = (f16[32,1152]{1,0:T(8,128)(2,1)S(1)}, f16[32,1152]{1,0:T(8,128)(2,1)S(1)}, u32[]{:S(2)}, u32[]{:S(2)}) collective-permute-start(f16[32,1152]{1,0:T(8,128)(2,1)S(1)} %convert_element_type.52), channel_id=1, source_target_pairs={{0,2},{1,3},{2,0},{3,1},{4,6},{5,7},{6,4},{7,5},{8,10},{9,11},{10,... | collective-permute-start | bytes 221192 | tf_op jit(solution)/shard_map/ppermute | solution.py:481
  24.1 3.1 %fetch.2 = (f32[28,4,128,128]{3,2,1,0:T(8,128)S(1)}, bf16[128,4096]{1,0:T(8,128)(2,1)S(1)}) custom-call(f32[2,28,4,128,128]{4,3,2,1,0:T(8,128)} %refs_0_.5, f32[32,1024]{1,0:T(8,128)S(1)} %get-tuple-element.60.refs_1_.refs_2_), custom_call_target="tpu_custom_call" | custom-call | flops 14680064 | bytes 14680064 | tf_op jit(solution)/shard_map/fetch/pallas_call | solution.py:59
  27.3 0.6 collective-permute-done.3
  28.0 1.8 %cell.2 = (bf16[32,512]{1,0:T(8,128)(2,1)S(1)}, f32[1,28,4,128]{3,2,1,0:T(4,128)S(1)}, f32[1,4,28]{2,1,0:T(4,128)S(1)}, f32[4,32,128]{2,1,0:T(8,128)S(1)}, f32[4...) custom-call(f32[32,1152]{1,0:T(8,128)S(1)} %get-tuple-element.52.refs_0_, f32[32,1152]{1,0:T(8,128)S(1)} %convert_element_type.53.refs_1_, ...), custom_call_target="tpu_custom_call" | custom-call | flops 7340032 | bytes 1048576 | tf_op jit(solution)/shard_map/cell/pallas_call | solution.py:367
  30.0 1.2 %collective-permute-start.5 = (bf16[32,512]{1,0:T(8,128)(2,1)S(1)}, bf16[32,512]{1,0:T(8,128)(2,1)S(1)}, u32[]{:S(2)}, u32[]{:S(2)}) collective-permute-start(bf16[32,512]{1,0:T(8,128)(2,1)S(1)} %get-tuple-element.64.refs_1_.refs_0_), channel_id=1, source_target_pairs={{0,2},{1,3},{2,0},{3,1},{4,6},{5,7},{6,4},{7,5},{8,10},{9,11},{10,... | collective-permute-start | bytes 98312 | tf_op jit(solution)/shard_map/ppermute | solution.py:481
  31.7 3.1 %fetch.3.refs_4_.refs_8_.matrix = f32[28,4,128,128]{3,2,1,0:T(8,128)S(1)} custom-call(f32[2,28,4,128,128]{4,3,2,1,0:T(8,128)} %refs_0_.5, bf16[32,512]{1,0:T(8,128)(2,1)S(1)} %get-tuple-element.64.refs_1_.refs_0_), custom_call_target="tpu_custom_call" | custom-call | flops 14680064 | bytes 14680064 | tf_op jit(solution)/shard_map/fetch/pallas_call | solution.py:59
  35.3 12.7 %all_to_all.21 = f16[8,16,1024]{2,1,0:T(8,128)(2,1)S(1)} all-to-all(f16[8,16,1024]{2,1,0:T(8,128)(2,1)S(1)} %bitcast.13), channel_id=1, replica_groups=mesh['tp'=8,'dp'=4] {'tp'}, dimensions={0} | all-to-all | bytes 524288 | tf_op jit(solution)/shard_map/all_to_all | solution.py:535
  48.1 12.0 %all_to_all.22.x = bf16[8,16,1024]{2,1,0:T(8,128)(2,1)S(1)} all-to-all(bf16[8,16,1024]{2,1,0:T(8,128)(2,1)S(1)} %broadcast_in_dim.2), channel_id=1, replica_groups=mesh['tp'=8,'dp'=4] {'tp'}, dimensions={0} | all-to-all | bytes 524288 | tf_op jit(solution)/shard_map/all_to_all | solution.py:538
  60.1 0.8 project_first.3
  62.7 1.3 %collective-permute-start.8 = (f16[32,1152]{1,0:T(8,128)(2,1)S(1)}, f16[32,1152]{1,0:T(8,128)(2,1)S(1)}, u32[]{:S(2)}, u32[]{:S(2)}) collective-permute-start(f16[32,1152]{1,0:T(8,128)(2,1)S(1)} %convert_element_type.60), channel_id=1, source_target_pairs={{0,2},{1,3},{2,0},{3,1},{4,6},{5,7},{6,4},{7,5},{8,10},{9,11},{10,... | collective-permute-start | bytes 221192 | tf_op jit(solution)/shard_map/ppermute | solution.py:481
  64.1 0.8 collective-permute-start.10
  64.9 3.5 %update.2.refs_12_.rest_0_ = f32[2,28,4,128,128]{4,3,2,1,0:T(8,128)} custom-call(f32[4,32,128]{2,1,0:T(8,128)S(1)} %get-tuple-element.77.kw, f32[4,32,128]{2,1,0:T(8,128)S(1)} %get-tuple-element.78.v, f32[4,32,128]{2,1,0:T(8,128)S(1)} %get-tuple-element.79.dec, f32[28,4,128,128]{3,2,1,0:T(8,128)S(1)} %get-tuple-element.62.refs_8_.refs_10_.matrix, ...), custom_call_target="tpu_custom_call" | custom-call | flops 14680064 | bytes 7340032 | tf_op jit(solution)/shard_map/update/pallas_call | solution.py:431
  68.5 1.8 %cell.3 = (bf16[32,512]{1,0:T(8,128)(2,1)S(1)}, f32[2,28,4,128]{3,2,1,0:T(4,128)S(1)}, f32[2,4,28]{2,1,0:T(4,128)S(1)}, f32[4,32,128]{2,1,0:T(8,128)S(1)}, f32[4...) custom-call(f32[32,1152]{1,0:T(8,128)S(1)} %get-tuple-element.67.refs_0_, f32[32,1152]{1,0:T(8,128)S(1)} %convert_element_type.61.refs_1_, ...), custom_call_target="tpu_custom_call" | custom-call | flops 7340032 | bytes 1048576 | tf_op jit(solution)/shard_map/cell/pallas_call | solution.py:367
  70.8 0.9 collective-permute-start.12
  72.2 3.5 %update.3.refs_4_ = f32[2,28,4,128,128]{4,3,2,1,0:T(8,128)} custom-call(f32[4,32,128]{2,1,0:T(8,128)S(1)} %get-tuple-element.81.kw, f32[4,32,128]{2,1,0:T(8,128)S(1)} %get-tuple-element.82.v, f32[4,32,128]{2,1,0:T(8,128)S(1)} %get-tuple-element.83.dec, f32[28,4,128,128]{3,2,1,0:T(8,128)S(1)} %fetch.3.refs_4_.refs_8_.matrix, ...), custom_call_target="tpu_custom_call", output_to_operand_aliasing={{}: (5, {})} | custom-call | flops 14680064 | bytes 7340032 | tf_op jit(solution)/shard_map/update/pallas_call | solution.py:431
  76.1 0.7 convert_element_type.64
  76.9 3.6 %all-to-all-start.3 = ((f16[8,16,1024]{2,1,0:T(8,128)(2,1)}), f16[8,16,1024]{2,1,0:T(8,128)(2,1)S(1)}, u32[]{:S(2)}, u32[]{:S(2)}) async-start(f16[8,16,1024]{2,1,0:T(8,128)(2,1)} %bitcast.4), calls=%async_computation.3 | async-start | bytes 524288 | tf_op jit(solution)/shard_map/all_to_all | solution.py:535
  80.4 0.6 copy.20
  81.0 0.6 copy.19
  81.7 7.9 %all-to-all-done.3 = f16[8,16,1024]{2,1,0:T(8,128)(2,1)S(1)} async-done(((f16[8,16,1024]{2,1,0:T(8,128)(2,1)}), f16[8,16,1024]{2,1,0:T(8,128)(2,1)S(1)}, u32[]{:S(2)}, u32[]{:S(2)}) %all-to-all-start.3) | async-done | bytes 262176 | tf_op jit(solution)/shard_map/all_to_all | solution.py:535
  89.6 0.6 fusion
  (65 shorter events, 7.1 us)
Async XLA Ops:
  20.0 1.6 %collective-permute-start = (f32[64,1152]{1,0:T(8,128)S(1)}, f32[64,1152]{1,0:T(8,128)S(1)}, u32[]{:S(2)}, u32[]{:S(2)}) collective-permute-start(f32[64,1152]{1,0:T(8,128)S(1)} %get-tuple-element.51), channel_id=1, source_target_pairs={{0,1},{1,0},{2,3},{3,2},{4,5},{5,4},{6,7},{7,6},{8,9},{9,8},{10,11... | collective-permute-start | bytes 884744 | tf_op jit(solution)/shard_map/ppermute | solution.py:481
  20.5 2.9 %collective-permute-start.2 = (f32[64,1024]{1,0:T(8,128)S(1)}, f32[64,1024]{1,0:T(8,128)S(1)}, u32[]{:S(2)}, u32[]{:S(2)}) collective-permute-start(f32[64,1024]{1,0:T(8,128)S(1)} %get-tuple-element.58), channel_id=1, source_target_pairs={{0,1},{1,0},{2,3},{3,2},{4,5},{5,4},{6,7},{7,6},{8,9},{9,8},{10,11... | collective-permute-start | bytes 786440 | tf_op jit(solution)/shard_map/ppermute | solution.py:481
  21.9 6.0 %collective-permute-start.1 = (f16[32,1152]{1,0:T(8,128)(2,1)S(1)}, f16[32,1152]{1,0:T(8,128)(2,1)S(1)}, u32[]{:S(2)}, u32[]{:S(2)}) collective-permute-start(f16[32,1152]{1,0:T(8,128)(2,1)S(1)} %convert_element_type.52), channel_id=1, source_target_pairs={{0,2},{1,3},{2,0},{3,1},{4,6},{5,7},{6,4},{7,5},{8,10},{9,11},{10,... | collective-permute-start | bytes 221192 | tf_op jit(solution)/shard_map/ppermute | solution.py:481
  23.6 4.3 %collective-permute-start.3 = (f16[32,1024]{1,0:T(8,128)(2,1)S(1)}, f16[32,1024]{1,0:T(8,128)(2,1)S(1)}, u32[]{:S(2)}, u32[]{:S(2)}) collective-permute-start(f16[32,1024]{1,0:T(8,128)(2,1)S(1)} %convert_element_type.54), channel_id=1, source_target_pairs={{0,2},{1,3},{2,0},{3,1},{4,6},{5,7},{6,4},{7,5},{8,10},{9,11},{10,... | collective-permute-start | bytes 196616 | tf_op jit(solution)/shard_map/ppermute | solution.py:481
  24.1 3.8 %copy-start.9 = (f32[2,28,4]{1,2,0:T(4,128)S(1)}, f32[2,28,4]{1,2,0:T(4,128)}, u32[]{:S(2)}) copy-start(f32[2,28,4]{1,2,0:T(4,128)} %param.25) | copy-start | bytes 2692
  24.1 3.8 %copy-start.10 = (f32[2,4]{1,0:T(2,128)S(1)}, f32[2,4]{1,0:T(2,128)}, u32[]{:S(2)}) copy-start(f32[2,4]{1,0:T(2,128)} %refs_4_.3) | copy-start | bytes 100
  29.8 5.1 %copy-start = (bf16[2,512,1024]{2,1,0:T(8,128)(2,1)S(1)}, bf16[2,512,1024]{2,1,0:T(8,128)(2,1)}, u32[]{:S(2)}) copy-start(bf16[2,512,1024]{2,1,0:T(8,128)(2,1)} %w.3) | copy-start | bytes 6291460
  29.8 5.1 %collective-permute-start.6 = (bf16[32,512]{1,0:T(8,128)(2,1)S(1)}, bf16[32,512]{1,0:T(8,128)(2,1)S(1)}, u32[]{:S(2)}, u32[]{:S(2)}) collective-permute-start(bf16[32,512]{1,0:T(8,128)(2,1)S(1)} %get-tuple-element.64.refs_1_.refs_0_), channel_id=1, source_target_pairs={{0,3},{1,2},{2,1},{3,0},{4,7},{5,6},{6,5},{7,4},{8,11},{9,10},{10,... | collective-permute-start | bytes 98312 | tf_op jit(solution)/shard_map/ppermute | solution.py:481
  30.0 4.9 %collective-permute-start.5 = (bf16[32,512]{1,0:T(8,128)(2,1)S(1)}, bf16[32,512]{1,0:T(8,128)(2,1)S(1)}, u32[]{:S(2)}, u32[]{:S(2)}) collective-permute-start(bf16[32,512]{1,0:T(8,128)(2,1)S(1)} %get-tuple-element.64.refs_1_.refs_0_), channel_id=1, source_target_pairs={{0,2},{1,3},{2,0},{3,1},{4,6},{5,7},{6,4},{7,5},{8,10},{9,11},{10,... | collective-permute-start | bytes 98312 | tf_op jit(solution)/shard_map/ppermute | solution.py:481
  31.2 3.7 %collective-permute-start.4 = (bf16[32,512]{1,0:T(8,128)(2,1)S(1)}, bf16[32,512]{1,0:T(8,128)(2,1)S(1)}, u32[]{:S(2)}, u32[]{:S(2)}) collective-permute-start(bf16[32,512]{1,0:T(8,128)(2,1)S(1)} %get-tuple-element.64.refs_1_.refs_0_), channel_id=1, source_target_pairs={{0,1},{1,0},{2,3},{3,2},{4,5},{5,4},{6,7},{7,6},{8,9},{9,8},{10,11... | collective-permute-start | bytes 98312 | tf_op jit(solution)/shard_map/ppermute | solution.py:481
  34.8 25.2 %copy-start.3 = (bf16[2,1024,512]{2,1,0:T(8,128)(2,1)S(1)}, bf16[2,1024,512]{2,1,0:T(8,128)(2,1)}, u32[]{:S(2)}) copy-start(bf16[2,1024,512]{2,1,0:T(8,128)(2,1)} %wq.1) | copy-start | bytes 6291460
  34.8 25.2 %copy-start.4 = (bf16[2,1024,512]{2,1,0:T(8,128)(2,1)S(1)}, bf16[2,1024,512]{2,1,0:T(8,128)(2,1)}, u32[]{:S(2)}) copy-start(bf16[2,1024,512]{2,1,0:T(8,128)(2,1)} %wk.1) | copy-start | bytes 6291460
  34.8 25.2 %copy-start.5 = (bf16[2,1024,32]{1,2,0:T(8,128)(2,1)S(1)}, bf16[2,1024,32]{1,2,0:T(8,128)(2,1)}, u32[]{:S(2)}) copy-start(bf16[2,1024,32]{1,2,0:T(8,128)(2,1)} %param.18) | copy-start | bytes 393220
  34.8 25.2 %copy-start.6 = (bf16[2,1024,32]{1,2,0:T(8,128)(2,1)S(1)}, bf16[2,1024,32]{1,2,0:T(8,128)(2,1)}, u32[]{:S(2)}) copy-start(bf16[2,1024,32]{1,2,0:T(8,128)(2,1)} %param.19) | copy-start | bytes 393220
  34.8 26.1 %copy-start.1 = (bf16[2,1024,512]{2,1,0:T(8,128)(2,1)S(1)}, bf16[2,1024,512]{2,1,0:T(8,128)(2,1)}, u32[]{:S(2)}) copy-start(bf16[2,1024,512]{2,1,0:T(8,128)(2,1)} %wv.1) | copy-start | bytes 6291460
  34.9 26.1 %copy-start.2 = (bf16[2,1024,512]{2,1,0:T(8,128)(2,1)S(1)}, bf16[2,1024,512]{2,1,0:T(8,128)(2,1)}, u32[]{:S(2)}) copy-start(bf16[2,1024,512]{2,1,0:T(8,128)(2,1)} %wo.1) | copy-start | bytes 6291460
  60.8 1.6 %collective-permute-start.7 = (f32[64,1152]{1,0:T(8,128)S(1)}, f32[64,1152]{1,0:T(8,128)S(1)}, u32[]{:S(2)}, u32[]{:S(2)}) collective-permute-start(f32[64,1152]{1,0:T(8,128)S(1)} %get-tuple-element.66), channel_id=1, source_target_pairs={{0,1},{1,0},{2,3},{3,2},{4,5},{5,4},{6,7},{7,6},{8,9},{9,8},{10,11... | collective-permute-start | bytes 884744 | tf_op jit(solution)/shard_map/ppermute | solution.py:481
  61.4 2.6 %collective-permute-start.9 = (f32[64,1024]{1,0:T(8,128)S(1)}, f32[64,1024]{1,0:T(8,128)S(1)}, u32[]{:S(2)}, u32[]{:S(2)}) collective-permute-start(f32[64,1024]{1,0:T(8,128)S(1)} %get-tuple-element.71), channel_id=1, source_target_pairs={{0,1},{1,0},{2,3},{3,2},{4,5},{5,4},{6,7},{7,6},{8,9},{9,8},{10,11... | collective-permute-start | bytes 786440 | tf_op jit(solution)/shard_map/ppermute | solution.py:481
  62.7 5.8 %collective-permute-start.8 = (f16[32,1152]{1,0:T(8,128)(2,1)S(1)}, f16[32,1152]{1,0:T(8,128)(2,1)S(1)}, u32[]{:S(2)}, u32[]{:S(2)}) collective-permute-start(f16[32,1152]{1,0:T(8,128)(2,1)S(1)} %convert_element_type.60), channel_id=1, source_target_pairs={{0,2},{1,3},{2,0},{3,1},{4,6},{5,7},{6,4},{7,5},{8,10},{9,11},{10,... | collective-permute-start | bytes 221192 | tf_op jit(solution)/shard_map/ppermute | solution.py:481
  64.1 4.4 %collective-permute-start.10 = (f16[32,1024]{1,0:T(8,128)(2,1)S(1)}, f16[32,1024]{1,0:T(8,128)(2,1)S(1)}, u32[]{:S(2)}, u32[]{:S(2)}) collective-permute-start(f16[32,1024]{1,0:T(8,128)(2,1)S(1)} %convert_element_type.62), channel_id=1, source_target_pairs={{0,2},{1,3},{2,0},{3,1},{4,6},{5,7},{6,4},{7,5},{8,10},{9,11},{10,... | collective-permute-start | bytes 196616 | tf_op jit(solution)/shard_map/ppermute | solution.py:481
  70.3 5.5 %collective-permute-start.13 = (bf16[32,512]{1,0:T(8,128)(2,1)S(1)}, bf16[32,512]{1,0:T(8,128)(2,1)S(1)}, u32[]{:S(2)}, u32[]{:S(2)}) collective-permute-start(bf16[32,512]{1,0:T(8,128)(2,1)S(1)} %get-tuple-element.80.refs_0_), channel_id=1, source_target_pairs={{0,3},{1,2},{2,1},{3,0},{4,7},{5,6},{6,5},{7,4},{8,11},{9,10},{10,... | collective-permute-start | bytes 98312 | tf_op jit(solution)/shard_map/ppermute | solution.py:481
  70.8 5.0 %collective-permute-start.12 = (bf16[32,512]{1,0:T(8,128)(2,1)S(1)}, bf16[32,512]{1,0:T(8,128)(2,1)S(1)}, u32[]{:S(2)}, u32[]{:S(2)}) collective-permute-start(bf16[32,512]{1,0:T(8,128)(2,1)S(1)} %get-tuple-element.80.refs_0_), channel_id=1, source_target_pairs={{0,2},{1,3},{2,0},{3,1},{4,6},{5,7},{6,4},{7,5},{8,10},{9,11},{10,... | collective-permute-start | bytes 98312 | tf_op jit(solution)/shard_map/ppermute | solution.py:481
  71.7 4.1 %collective-permute-start.11 = (bf16[32,512]{1,0:T(8,128)(2,1)S(1)}, bf16[32,512]{1,0:T(8,128)(2,1)S(1)}, u32[]{:S(2)}, u32[]{:S(2)}) collective-permute-start(bf16[32,512]{1,0:T(8,128)(2,1)S(1)} %get-tuple-element.80.refs_0_), channel_id=1, source_target_pairs={{0,1},{1,0},{2,3},{3,2},{4,5},{5,4},{6,7},{7,6},{8,9},{9,8},{10,11... | collective-permute-start | bytes 98312 | tf_op jit(solution)/shard_map/ppermute | solution.py:481
  76.9 12.7 %all-to-all-start.3 = ((f16[8,16,1024]{2,1,0:T(8,128)(2,1)}), f16[8,16,1024]{2,1,0:T(8,128)(2,1)S(1)}, u32[]{:S(2)}, u32[]{:S(2)}) async-start(f16[8,16,1024]{2,1,0:T(8,128)(2,1)} %bitcast.4), calls=%async_computation.3 | async-start | bytes 524288 | tf_op jit(solution)/shard_map/all_to_all | solution.py:535
  (2 other events, 7.6 us)
